TPU v7x, 32 devices: a whole 2x2x4 slice. The times are simulated.
32 devices in a mesh: dp: 4 (over y, x), kv: 4 (over z), tp: 2 (over core).
Axes of the slice: x: 2, y: 2, z: 4, core: 2. Of those that a mesh axis runs over, the one named last changes fastest.
Arguments:
- tokens: bfloat16 [4096, 2048], P(('dp', 'kv'), 'tp'), parts along dimension 0, may hold values from -6 to 6
- query_weight: bfloat16 [2048, 1024], P(None, 'tp'), may hold values from -2 to 2
- key_weight: bfloat16 [2048, 1024], P(None, 'tp'), may hold values from -2 to 2
- value_weight: bfloat16 [2048, 1024], P(None, 'tp'), may hold values from -0.125 to 0.125
- out_weight: bfloat16 [1024, 2048], P(None, 'tp'), may hold values from -0.75 to 0.75
- chosen: int32 [128, 16], P(('dp', 'kv')), parts along dimension 0, may hold values from -1 to 31, as said below
Outputs:
- mixed: bfloat16 [4096, 2048], P(('dp', 'kv'), 'tp'), parts along dimension 0
There are 4 independent parts, one for each index of `dp`. A program takes and returns all parts, laid end to end along the dimension named above; an argument that names none is the same for every part. Nothing has to cross between parts.
Inputs may be any that keep to these rules, and one draw needn't show every extreme that they name: Each row of chosen lists distinct key blocks no later than its own query block, followed or mixed with -1 for empty slots; the own block is always listed, and block 0 too. For the 8 query blocks of one index of kv (aligned runs of rows), the distinct listed key blocks that lie among the 8 blocks of any one other index number at most 3, and exactly 3 for the index just before.
All inputs are finite; a program needn't handle non-finite values.
Results may differ from a plain program's by a relative error of at most 0.0084.
Values may be sent and summed in bfloat16 or wider, within the bound.
A program may use at most 128 MiB of HBM per device.

v0:
```python
import functools

import jax
import jax.numpy as jnp
import numpy as np
from jax import lax
from jax.experimental import pallas as pl
from jax.experimental.pallas import tpu as pltpu
from jax.sharding import PartitionSpec as P

HEAD_DIM = 64
BLOCK = 32
CAP = 3
LANES = 128
ROTARY_BASE = 500000.0
MASKED = -1e30
MESH = pl.DeviceIdType.MESH
F32 = jnp.float32
BF16 = jnp.bfloat16


def rotary_tables(rows, devices):
    half = HEAD_DIM // 2
    inverse = (1.0 / ROTARY_BASE ** (np.arange(half, dtype=np.float64) / half))
    lanes = np.tile(inverse, LANES // half)[None, :]
    row_angle = np.arange(rows, dtype=np.float64)[:, None] * lanes
    base_angle = (np.arange(devices, dtype=np.float64) * rows)[:, None] * lanes
    pack = lambda a: np.concatenate([np.cos(a), np.sin(a)], axis=1).astype(np.float32)
    return pack(row_angle), pack(base_angle)


def listed_columns(chosen, holder, rows):
    blocks = rows // BLOCK
    ids = holder * blocks + lax.broadcasted_iota(jnp.int32, (blocks, rows), 1) // BLOCK
    hit = jnp.zeros((blocks, rows), F32)
    for slot in range(chosen.shape[1]):
        hit = jnp.where(chosen[:, slot : slot + 1] == ids, 1.0, hit)
    return hit


def selection(hit, earlier):
    blocks, rows = hit.shape
    need = jnp.broadcast_to(jnp.max(hit, axis=0, keepdims=True), hit.shape)
    rank = jnp.dot(need.astype(BF16), earlier, preferred_element_type=F32)
    shape = (CAP * BLOCK, rows)
    slot_row = lax.broadcasted_iota(jnp.int32, shape, 0)
    column = lax.broadcasted_iota(jnp.int32, shape, 1)
    wanted = (slot_row // BLOCK).astype(F32)
    place = jnp.where(need[:1] > 0.5, rank[:1], -1.0)
    same = (slot_row % BLOCK) == (column % BLOCK)
    return jnp.where(same & (place == wanted), 1.0, 0.0).astype(BF16)


def layer(
    devices,
    chosen_hbm, base_hbm, row_hbm, tok_hbm, wq_hbm, wk_hbm, wv_hbm, wo_hbm,
    out_ref,
    chosen_ref, base_ref, tab, tok_own, tok_peer, wq, wk, wv, wo, q_acc, k_acc, v_acc, k_own, v_own, q2,
    lists, picks, k_rows, v_rows, raw, widest, peak, total, summed, weigh, att_own, att_peer,
    load_sem, tok_sem, att_sem, list_send, list_recv, key_send, key_recv, root_send, root_recv,
):
    me = lax.axis_index("kv")
    core = lax.axis_index("tp")
    rows, half = tok_own.shape
    head_width = k_own.shape[1]
    pairs = head_width // LANES
    picked = CAP * BLOCK
    other = 1 - core

    loads = [
        pltpu.make_async_copy(src, dst, load_sem.at[i])
        for i, (src, dst) in enumerate(
            ((chosen_hbm, chosen_ref), (base_hbm, base_ref), (tok_hbm, tok_own), (wk_hbm, wk), (row_hbm, tab), (wv_hbm, wv), (wq_hbm, wq), (wo_hbm, wo))
        )
    ]
    for load in loads:
        load.start()
    chosen_load, base_load, tok_load, wk_load, tab_load, wv_load, wq_load, wo_load = loads

    barrier = pltpu.get_barrier_semaphore()
    pl.semaphore_signal(barrier, inc=1, device_id={"tp": other}, device_id_type=MESH)

    def greet(d, _):
        pl.semaphore_signal(
            barrier, inc=1, device_id={"kv": lax.rem(me + d, devices)}, device_id_type=MESH
        )
        return 0

    lax.fori_loop(1, devices, greet, 0)

    own_half = pl.ds(pl.multiple_of(core * half, half), half)
    peer_half = pl.ds(pl.multiple_of(other * half, half), half)

    tok_load.wait()
    wk_load.wait()
    k_acc[...] = jnp.dot(tok_own[...], wk[own_half, :], preferred_element_type=F32)

    pl.semaphore_wait(barrier, devices)

    def list_copy(d, target):
        return pltpu.make_async_remote_copy(
            src_ref=chosen_ref, dst_ref=lists.at[d], send_sem=list_send.at[d],
            recv_sem=list_recv.at[d], device_id={"kv": target}, device_id_type=MESH,
        )

    def send_list(d, _):
        list_copy(d, me - d).start()
        return 0

    chosen_load.wait()
    lax.fori_loop(1, me + 1, send_list, 0)
    tok_copy = pltpu.make_async_remote_copy(
        src_ref=tok_own, dst_ref=tok_peer, send_sem=tok_sem.at[0], recv_sem=tok_sem.at[1],
        device_id={"tp": other}, device_id_type=MESH,
    )
    tok_copy.start()

    wv_load.wait()
    v_acc[...] = jnp.dot(tok_own[...], wv[own_half, :], preferred_element_type=F32)
    wq_load.wait()
    q_acc[...] = jnp.dot(tok_own[...], wq[own_half, :], preferred_element_type=F32)

    tab_load.wait()
    base_load.wait()
    lane = lax.broadcasted_iota(jnp.int32, (rows, LANES), 1)
    first = (lane % HEAD_DIM) < HEAD_DIM // 2
    base = base_ref[pl.ds(me, 1), :]
    row_cos, row_sin = tab[:, :LANES], tab[:, LANES:]
    base_cos, base_sin = base[:, :LANES], base[:, LANES:]
    cosine = row_cos * base_cos - row_sin * base_sin
    sine = row_sin * base_cos + row_cos * base_sin
    sine = jnp.where(first, -sine, sine)
    tab[:, :LANES] = cosine
    tab[:, LANES:] = sine

    def rotated(x):
        swapped = jnp.where(
            first,
            pltpu.roll(x, LANES - HEAD_DIM // 2, axis=1),
            pltpu.roll(x, HEAD_DIM // 2, axis=1),
        )
        return x * tab[:, :LANES] + swapped * tab[:, LANES:]

    row_i = lax.broadcasted_iota(jnp.int32, (rows, rows), 0)
    col_i = lax.broadcasted_iota(jnp.int32, (rows, rows), 1)
    earlier = jnp.where((row_i % BLOCK == 0) & (row_i // BLOCK < col_i // BLOCK), 1.0, 0.0).astype(BF16)

    tok_copy.wait_recv()
    k_full = k_acc[...] + jnp.dot(tok_peer[...], wk[peer_half, :], preferred_element_type=F32)
    for i in range(pairs):
        tile = slice(i * LANES, (i + 1) * LANES)
        k_own[:, tile] = rotated(k_full[:, tile]).astype(BF16)

    buffers = ((k_own, k_rows), (v_own, v_rows))

    def row_copy(kind, d, target, holder):
        buffer = buffers[kind][1]

        def part(span):
            return pltpu.make_async_remote_copy(
                src_ref=buffer.at[lax.rem(me + d, devices), span], dst_ref=buffer.at[d, span],
                send_sem=key_send.at[kind, d], recv_sem=key_recv.at[kind, d],
                device_id={"kv": target}, device_id_type=MESH,
            )

        return part(slice(BLOCK, picked)), part(slice(0, picked)), holder == 0

    def each(copies, act):
        short, whole, is_short = copies
        pl.when(is_short)(lambda: act(short))
        pl.when(jnp.logical_not(is_short))(lambda: act(whole))

    relayed = devices > 2
    direct = devices - 2 if relayed else devices - 1
    relay_here = (me == devices - 2) if relayed else False

    def root_copy(kind, d, passing=False):
        own, buffer = buffers[kind]
        block = slice(0, BLOCK)
        return pltpu.make_async_remote_copy(
            src_ref=buffer.at[me, block] if passing else own.at[block], dst_ref=buffer.at[d, block],
            send_sem=root_send.at[kind, d], recv_sem=root_recv.at[kind],
            device_id={"kv": lax.rem(d, devices)}, device_id_type=MESH,
        )

    def send_root(kind):
        @pl.when(me == 0)
        def _():
            def one(step, _):
                root_copy(kind, direct - step).start()
                return 0

            lax.fori_loop(0, direct, one, 0)

    def arrived(kind, d):
        each(row_copy(kind, d, me, me - d), lambda c: c.wait_recv())

        @pl.when((d == me) & jnp.logical_not(relay_here))
        def _():
            root_copy(kind, d).wait_recv()

    send_root(0)

    def send_keys(d, _):
        list_copy(d, me).wait_recv()
        pick = selection(listed_columns(lists[d], me, rows), earlier)
        picks[d] = pick
        k_rows[me + d] = jnp.dot(pick, k_own[...], preferred_element_type=F32).astype(BF16)
        each(row_copy(0, d, me + d, me), lambda c: c.start())
        return 0

    lax.fori_loop(1, devices - me, send_keys, 0)

    v_own[...] = (
        v_acc[...] + jnp.dot(tok_peer[...], wv[peer_half, :], preferred_element_type=F32)
    ).astype(BF16)

    send_root(1)

    def send_values(step, _):
        d = devices - 1 - me - step
        v_rows[me + d] = jnp.dot(picks[d], v_own[...], preferred_element_type=F32).astype(BF16)
        each(row_copy(1, d, me + d, me), lambda c: c.start())
        return 0

    lax.fori_loop(0, devices - 1 - me, send_values, 0)

    q_full = q_acc[...] + jnp.dot(tok_peer[...], wq[peer_half, :], preferred_element_type=F32)
    for i in range(pairs):
        tile = slice(i * LANES, (i + 1) * LANES)
        q = rotated(q_full[:, tile]).astype(BF16).astype(F32) * (HEAD_DIM**-0.5)
        q2[i, :rows, :] = jnp.where(lane < HEAD_DIM, q, 0.0).astype(BF16)
        q2[i, rows:, :] = jnp.where(lane < HEAD_DIM, 0.0, q).astype(BF16)

    chosen = chosen_ref[...]

    def spread(hit):
        keys = hit.shape[1]
        blocks = hit.shape[0]
        wide = jnp.broadcast_to(hit[:, None, :], (blocks, BLOCK, keys))
        return wide.reshape(blocks * BLOCK, keys)

    def scores_of(i, keys):
        return lax.dot_general(
            q2[i], keys, (((1,), (1,)), ((), ())), preferred_element_type=F32
        )

    def gauge(d, _):
        hit = listed_columns(chosen, me - d, rows)
        pick = selection(hit, earlier)
        got = lax.dot_general(
            hit.astype(BF16), pick, (((1,), (1,)), ((), ())), preferred_element_type=F32
        )
        far = jnp.where(spread(got) > 0.5, 0.0, MASKED)
        far = jnp.concatenate([far, far], axis=0)
        arrived(0, d)
        for i in range(pairs):
            tile = slice(i * LANES, (i + 1) * LANES)
            scores = scores_of(i, k_rows[d, :, tile]) + far
            raw[d - 1, i] = scores
            widest[i] = jnp.maximum(widest[i], scores)
        return 0

    listed = spread(listed_columns(chosen, me, rows))
    bias = jnp.where((listed > 0.5) & (col_i <= row_i), 0.0, MASKED)
    bias = jnp.concatenate([bias, bias], axis=0)
    for i in range(pairs):
        tile = slice(i * LANES, (i + 1) * LANES)
        scores = scores_of(i, k_own[:, tile]) + bias
        top = jnp.max(scores, axis=1, keepdims=True)
        weights = jnp.exp(scores - top)
        peak[i] = jnp.broadcast_to(top, peak.shape[1:])
        total[i] = sum(weights[:, j : j + LANES] for j in range(0, rows, LANES))
        summed[i] = jnp.dot(weights.astype(BF16), v_own[:, tile], preferred_element_type=F32)
        widest[i] = jnp.full(widest.shape[1:], MASKED, F32)

    if relayed:

        @pl.when(relay_here)
        def _():
            for kind in range(2):
                root_copy(kind, me).wait_recv()
                root_copy(kind, devices - 1, True).start()

    lax.fori_loop(1, me + 1, gauge, 0)

    @pl.when(me > 0)
    def _():
        for i in range(pairs):
            old = peak[i]
            top = jnp.maximum(old, jnp.max(widest[i], axis=1, keepdims=True))
            factor = jnp.exp(old - top)
            peak[i] = top
            total[i] = total[i] * factor
            summed[i] = summed[i] * factor

    def attend(step, _):
        d = jnp.where(me == devices - 1, step, me + 1 - step)
        for i in range(pairs):
            weights = jnp.exp(raw[d - 1, i] - peak[i, :, :picked])
            total[i, :, :picked] += weights
            weigh[i] = weights.astype(BF16)
        arrived(1, d)
        for i in range(pairs):
            tile = slice(i * LANES, (i + 1) * LANES)
            summed[i] += jnp.dot(weigh[i], v_rows[d, :, tile], preferred_element_type=F32)
        return 0

    lax.fori_loop(1, me + 1, attend, 0)

    att_copies = []
    for i in range(pairs):
        ratio = summed[i] / jnp.sum(total[i], axis=1, keepdims=True)
        att_own[i] = jnp.where(lane < HEAD_DIM, ratio[:rows], ratio[rows:]).astype(BF16)
        att_copies.append(
            pltpu.make_async_remote_copy(
                src_ref=att_own.at[i], dst_ref=att_peer.at[i], send_sem=att_sem.at[0, i],
                recv_sem=att_sem.at[1, i], device_id={"tp": other}, device_id_type=MESH,
            )
        )
        att_copies[-1].start()
    wo_load.wait()
    own_rows = pl.ds(pl.multiple_of(core * head_width, head_width), head_width)
    peer_rows = pl.ds(pl.multiple_of(other * head_width, head_width), head_width)
    joined = lambda ref: jnp.concatenate([ref[i] for i in range(pairs)], axis=1)
    mixed = jnp.dot(joined(att_own), wo[own_rows, :], preferred_element_type=F32)
    for copy in att_copies:
        copy.wait_recv()
    mixed = mixed + jnp.dot(joined(att_peer), wo[peer_rows, :], preferred_element_type=F32)
    out_ref[...] = mixed.astype(BF16)

    for copy in att_copies:
        copy.wait_send()
    tok_copy.wait_send()

    def drain_list(d, _):
        list_copy(d, me - d).wait_send()
        return 0

    lax.fori_loop(1, me + 1, drain_list, 0)

    def drain_rows(d, _):
        each(row_copy(0, d, me + d, me), lambda c: c.wait_send())
        each(row_copy(1, d, me + d, me), lambda c: c.wait_send())
        return 0

    lax.fori_loop(1, devices - me, drain_rows, 0)

    @pl.when(me == 0)
    def _():
        def drain_root(d, _):
            root_copy(0, d).wait_send()
            root_copy(1, d).wait_send()
            return 0

        lax.fori_loop(1, direct + 1, drain_root, 0)

    if relayed:

        @pl.when(relay_here)
        def _():
            for kind in range(2):
                root_copy(kind, devices - 1, True).wait_send()


def on_device(devices, tokens, query_weight, key_weight, value_weight, out_weight, chosen):
    rows, half = tokens.shape
    width, head_width = query_weight.shape
    pairs = head_width // LANES
    picked = CAP * BLOCK
    row_table, base_table = rotary_tables(rows, devices)
    vmem = pl.BlockSpec(memory_space=pltpu.VMEM)
    anywhere = pl.BlockSpec(memory_space=pl.ANY)
    dma = pltpu.SemaphoreType.DMA
    return pl.pallas_call(
        functools.partial(layer, devices),
        out_shape=pltpu.VMEM((rows, out_weight.shape[1]), BF16),
        in_specs=[anywhere] * 8,
        out_specs=vmem,
        scratch_shapes=[
            pltpu.VMEM(chosen.shape, jnp.int32),
            pltpu.VMEM(base_table.shape, F32),
            pltpu.VMEM((rows, 2 * LANES), F32),
            pltpu.VMEM((rows, half), BF16),
            pltpu.VMEM((rows, half), BF16),
            pltpu.VMEM((width, head_width), BF16),
            pltpu.VMEM((width, head_width), BF16),
            pltpu.VMEM((width, head_width), BF16),
            pltpu.VMEM(out_weight.shape, BF16),
            pltpu.VMEM((rows, head_width), F32),
            pltpu.VMEM((rows, head_width), F32),
            pltpu.VMEM((rows, head_width), F32),
            pltpu.VMEM((rows, head_width), BF16),
            pltpu.VMEM((rows, head_width), BF16),
            pltpu.VMEM((pairs, 2 * rows, LANES), BF16),
            pltpu.VMEM((devices,) + chosen.shape, jnp.int32),
            pltpu.VMEM((devices, picked, rows), BF16),
            pltpu.VMEM((devices, picked, head_width), BF16),
            pltpu.VMEM((devices, picked, head_width), BF16),
            pltpu.VMEM((devices - 1, pairs, 2 * rows, picked), F32),
            pltpu.VMEM((pairs, 2 * rows, picked), F32),
            pltpu.VMEM((pairs, 2 * rows, LANES), F32),
            pltpu.VMEM((pairs, 2 * rows, LANES), F32),
            pltpu.VMEM((pairs, 2 * rows, LANES), F32),
            pltpu.VMEM((pairs, 2 * rows, picked), BF16),
            pltpu.VMEM((pairs, rows, LANES), BF16),
            pltpu.VMEM((pairs, rows, LANES), BF16),
            dma((8,)),
            dma((2,)),
            dma((2, pairs)),
            dma((devices,)),
            dma((devices,)),
            dma((2, devices)),
            dma((2, devices)),
            dma((2, devices)),
            dma((2,)),
        ],
        compiler_params=pltpu.CompilerParams(
            collective_id=0, has_side_effects=True, vmem_limit_bytes=62 * 1024 * 1024
        ),
        name="layer",
    )(
        chosen, jnp.asarray(base_table), jnp.asarray(row_table), tokens,
        query_weight, key_weight, value_weight, out_weight,
    )


def solution(mesh):
    placed = (
        P(("dp", "kv"), "tp"),
        P(None, "tp"),
        P(None, "tp"),
        P(None, "tp"),
        P(None, "tp"),
        P(("dp", "kv"), None),
    )
    return jax.shard_map(
        functools.partial(on_device, mesh.shape["kv"]),
        mesh=mesh, in_specs=placed, out_specs=P(("dp", "kv"), "tp"), check_vma=False,
    )
```

profile of v0, /device:TPU:17, one launch (start us, length us, event | category | flops | bytes accessed | tf_op | source)
XLA Modules:
  0.0 26.7 jit_solution(3026065839966293015)
XLA Ops:
  0.0 25.9 %layer.1 = bf16[256,1024]{1,0:T(8,128)(2,1)S(1)} custom-call(s32[8,16]{1,0:T(8,128)} %chosen_hbm.1, f32[4,256]{1,0:T(4,128)} %constant.4.clone.base_hbm, f32[256,256]{1,0:T(8,128)} %constant.5.clone.row_hbm, bf16[256,1024]{1,0:T(8,128)(2,1)} %tok_hbm.1, bf16[2048,512]{1,0:T(8,128)(2,1)} %wq_hbm.1, bf16[2048,512]{1,0:T(8,128)(2,1)} %wk_hbm.1, ...), custom_call_target="tpu_custom_call" | custom-call | tf_op jit(solution)/shard_map/layer/pallas_call | solution.py:375
  25.9 0.8 %copy.10 = bf16[256,1024]{1,0:T(8,128)(2,1)} copy(bf16[256,1024]{1,0:T(8,128)(2,1)S(1)} %layer.1) | data formatting | bytes 1048576
where the time goes:
time: 26.8 us; the launch traced here: 26.7 us
  Pallas kernels  25.9 us (97%)
  local copies, waits for them, and re-layouts  0.8 us (3%)
    pallas_call x1, Pallas kernels, on_device(): pl.pallas_call(functools.partial(layer, devices), out_shape=pltpu.VMEM((r...  25.9 us
    unnamed x1, local copies, waits for them, and re-layouts  0.8 us

commit v1 on v0

v1 whole, which is shorter than its diff:
```python
import functools

import jax
import jax.numpy as jnp
import numpy as np
from jax import lax
from jax.experimental import pallas as pl
from jax.experimental.pallas import tpu as pltpu
from jax.sharding import PartitionSpec as P

HEAD_DIM = 64
BLOCK = 32
CAP = 3
LANES = 128
ROTARY_BASE = 500000.0
MASKED = -1e30
MESH = pl.DeviceIdType.MESH
F32 = jnp.float32
BF16 = jnp.bfloat16


def rotary_tables(rows, devices):
    half = HEAD_DIM // 2
    inverse = (1.0 / ROTARY_BASE ** (np.arange(half, dtype=np.float64) / half))
    lanes = np.tile(inverse, LANES // half)[None, :]
    row_angle = np.arange(rows, dtype=np.float64)[:, None] * lanes
    base_angle = (np.arange(devices, dtype=np.float64) * rows)[:, None] * lanes
    pack = lambda a: np.concatenate([np.cos(a), np.sin(a)], axis=1).astype(np.float32)
    return pack(row_angle), pack(base_angle)


def listed_columns(chosen, holder, rows):
    blocks = rows // BLOCK
    ids = holder * blocks + lax.broadcasted_iota(jnp.int32, (blocks, rows), 1) // BLOCK
    hit = jnp.zeros((blocks, rows), F32)
    for slot in range(chosen.shape[1]):
        hit = jnp.where(chosen[:, slot : slot + 1] == ids, 1.0, hit)
    return hit


def selection(hit, earlier):
    blocks, rows = hit.shape
    need = jnp.broadcast_to(jnp.max(hit, axis=0, keepdims=True), hit.shape)
    rank = jnp.dot(need.astype(BF16), earlier, preferred_element_type=F32)
    shape = (CAP * BLOCK, rows)
    slot_row = lax.broadcasted_iota(jnp.int32, shape, 0)
    column = lax.broadcasted_iota(jnp.int32, shape, 1)
    wanted = (slot_row // BLOCK).astype(F32)
    place = jnp.where(need[:1] > 0.5, rank[:1], -1.0)
    same = (slot_row % BLOCK) == (column % BLOCK)
    return jnp.where(same & (place == wanted), 1.0, 0.0).astype(BF16)


def layer(
    devices,
    chosen_hbm, base_hbm, row_hbm, tok_hbm, wq_hbm, wk_hbm, wv_hbm, wo_hbm,
    out_ref,
    chosen_ref, base_ref, tab, tok_own, tok_peer, wq, wk, wv, wo, q_acc, k_acc, v_acc, k_own, v_own, q2,
    lists, picks, k_rows, v_rows, far, peak, total, summed, mixed, att_own, att_peer,
    load_sem, tok_sem, att_sem, list_send, list_recv, key_send, key_recv, root_send, root_recv, pass_send,
):
    me = lax.axis_index("kv")
    core = lax.axis_index("tp")
    rows, half = tok_own.shape
    head_width = k_own.shape[1]
    pairs = head_width // LANES
    picked = CAP * BLOCK
    other = 1 - core

    loads = [
        pltpu.make_async_copy(src, dst, load_sem.at[i])
        for i, (src, dst) in enumerate(
            ((chosen_hbm, chosen_ref), (tok_hbm, tok_own), (wk_hbm, wk), (base_hbm, base_ref), (row_hbm, tab), (wv_hbm, wv), (wq_hbm, wq), (wo_hbm, wo))
        )
    ]
    for load in loads:
        load.start()
    chosen_load, tok_load, wk_load, base_load, tab_load, wv_load, wq_load, wo_load = loads

    barrier = pltpu.get_barrier_semaphore()
    pl.semaphore_signal(barrier, inc=1, device_id={"tp": other}, device_id_type=MESH)

    def greet(d, _):
        pl.semaphore_signal(
            barrier, inc=1, device_id={"kv": lax.rem(me + d, devices)}, device_id_type=MESH
        )
        return 0

    lax.fori_loop(1, devices, greet, 0)

    own_half = pl.ds(pl.multiple_of(core * half, half), half)
    peer_half = pl.ds(pl.multiple_of(other * half, half), half)

    def list_copy(d, target):
        return pltpu.make_async_remote_copy(
            src_ref=chosen_ref, dst_ref=lists.at[d], send_sem=list_send.at[d],
            recv_sem=list_recv.at[d], device_id={"kv": target}, device_id_type=MESH,
        )

    def send_list(d, _):
        list_copy(d, me - d).start()
        return 0

    tok_copy = pltpu.make_async_remote_copy(
        src_ref=tok_own, dst_ref=tok_peer, send_sem=tok_sem.at[0], recv_sem=tok_sem.at[1],
        device_id={"tp": other}, device_id_type=MESH,
    )

    chosen_load.wait()
    tok_load.wait()
    pl.semaphore_wait(barrier, devices)
    lax.fori_loop(1, me + 1, send_list, 0)
    tok_copy.start()

    wk_load.wait()
    k_acc[...] = jnp.dot(tok_own[...], wk[own_half, :], preferred_element_type=F32)
    wv_load.wait()
    v_acc[...] = jnp.dot(tok_own[...], wv[own_half, :], preferred_element_type=F32)
    wq_load.wait()
    q_acc[...] = jnp.dot(tok_own[...], wq[own_half, :], preferred_element_type=F32)

    tab_load.wait()
    base_load.wait()
    lane = lax.broadcasted_iota(jnp.int32, (rows, LANES), 1)
    first = (lane % HEAD_DIM) < HEAD_DIM // 2
    base = base_ref[pl.ds(me, 1), :]
    row_cos, row_sin = tab[:, :LANES], tab[:, LANES:]
    base_cos, base_sin = base[:, :LANES], base[:, LANES:]
    cosine = row_cos * base_cos - row_sin * base_sin
    sine = row_sin * base_cos + row_cos * base_sin
    sine = jnp.where(first, -sine, sine)
    tab[:, :LANES] = cosine
    tab[:, LANES:] = sine

    def rotated(x):
        swapped = jnp.where(
            first,
            pltpu.roll(x, LANES - HEAD_DIM // 2, axis=1),
            pltpu.roll(x, HEAD_DIM // 2, axis=1),
        )
        return x * tab[:, :LANES] + swapped * tab[:, LANES:]

    row_i = lax.broadcasted_iota(jnp.int32, (rows, rows), 0)
    col_i = lax.broadcasted_iota(jnp.int32, (rows, rows), 1)
    earlier = jnp.where((row_i % BLOCK == 0) & (row_i // BLOCK < col_i // BLOCK), 1.0, 0.0).astype(BF16)

    def choose(d, _):
        list_copy(d, me).wait_recv()
        picks[d] = selection(listed_columns(lists[d], me, rows), earlier)
        return 0

    lax.fori_loop(1, devices - me, choose, 0)

    buffers = ((k_own, k_rows), (v_own, v_rows))

    def row_copy(kind, i, d, target, holder):
        buffer = buffers[kind][1]

        def part(span):
            return pltpu.make_async_remote_copy(
                src_ref=buffer.at[lax.rem(me + d, devices), i, span], dst_ref=buffer.at[d, i, span],
                send_sem=key_send.at[kind, i, d], recv_sem=key_recv.at[kind, i, d],
                device_id={"kv": target}, device_id_type=MESH,
            )

        return part(slice(BLOCK, picked)), part(slice(0, picked)), holder == 0

    def each(copies, act):
        short, whole, is_short = copies
        pl.when(is_short)(lambda: act(short))
        pl.when(jnp.logical_not(is_short))(lambda: act(whole))

    relayed = devices > 2
    direct = devices - 2 if relayed else devices - 1
    relay_here = (me == devices - 2) if relayed else False

    def root_copy(kind, i, d, passing=False):
        own, buffer = buffers[kind]
        block = slice(0, BLOCK)
        return pltpu.make_async_remote_copy(
            src_ref=buffer.at[me, i, block] if passing else own.at[block, i * LANES : (i + 1) * LANES],
            dst_ref=buffer.at[d, i, block],
            send_sem=pass_send.at[kind, i] if passing else root_send.at[kind, i, d],
            recv_sem=root_recv.at[kind, i],
            device_id={"kv": lax.rem(d, devices)}, device_id_type=MESH,
        )

    def send_root(kind, some):
        @pl.when(me == 0)
        def _():
            def one(step, _):
                for i in some:
                    root_copy(kind, i, direct - step).start()
                return 0

            lax.fori_loop(0, direct, one, 0)

    def send_rows(kind, some):
        own, buffer = buffers[kind]
        columns = slice(some[0] * LANES, (some[-1] + 1) * LANES)

        def one(d, _):
            got = jnp.dot(picks[d], own[:, columns], preferred_element_type=F32).astype(BF16)
            for n, i in enumerate(some):
                buffer[me + d, i] = got[:, n * LANES : (n + 1) * LANES]
            for i in some:
                each(row_copy(kind, i, d, me + d, me), lambda c: c.start())
            return 0

        lax.fori_loop(1, devices - me, one, 0)

    tok_copy.wait_recv()
    step_pairs = 2 if pairs % 2 == 0 else 1
    for start in range(0, pairs, step_pairs):
        some = list(range(start, start + step_pairs))
        columns = slice(start * LANES, (start + step_pairs) * LANES)
        k_full = k_acc[:, columns] + jnp.dot(tok_peer[...], wk[peer_half, columns], preferred_element_type=F32)
        for n, i in enumerate(some):
            k_own[:, i * LANES : (i + 1) * LANES] = rotated(k_full[:, n * LANES : (n + 1) * LANES]).astype(BF16)
        send_root(0, some)
        send_rows(0, some)
        v_own[:, columns] = (
            v_acc[:, columns] + jnp.dot(tok_peer[...], wv[peer_half, columns], preferred_element_type=F32)
        ).astype(BF16)
        send_root(1, some)
        send_rows(1, some)

    q_full = q_acc[...] + jnp.dot(tok_peer[...], wq[peer_half, :], preferred_element_type=F32)
    for i in range(pairs):
        tile = slice(i * LANES, (i + 1) * LANES)
        q = rotated(q_full[:, tile]).astype(BF16).astype(F32) * (HEAD_DIM**-0.5)
        q2[i, :rows, :] = jnp.where(lane < HEAD_DIM, q, 0.0).astype(BF16)
        q2[i, rows:, :] = jnp.where(lane < HEAD_DIM, 0.0, q).astype(BF16)

    chosen = chosen_ref[...]

    def spread(hit):
        keys = hit.shape[1]
        blocks = hit.shape[0]
        wide = jnp.broadcast_to(hit[:, None, :], (blocks, BLOCK, keys))
        return wide.reshape(blocks * BLOCK, keys)

    def scores_of(i, keys):
        return lax.dot_general(
            q2[i], keys, (((1,), (1,)), ((), ())), preferred_element_type=F32
        )

    listed = spread(listed_columns(chosen, me, rows))
    bias = jnp.where((listed > 0.5) & (col_i <= row_i), 0.0, MASKED)
    bias = jnp.concatenate([bias, bias], axis=0)
    for i in range(pairs):
        tile = slice(i * LANES, (i + 1) * LANES)
        scores = scores_of(i, k_own[:, tile]) + bias
        top = jnp.max(scores, axis=1, keepdims=True)
        weights = jnp.exp(scores - top)
        peak[i] = jnp.broadcast_to(top, peak.shape[1:])
        total[i] = sum(weights[:, j : j + LANES] for j in range(0, rows, LANES))
        summed[i] = jnp.dot(weights.astype(BF16), v_own[:, tile], preferred_element_type=F32)

    def gauge(d, _):
        hit = listed_columns(chosen, me - d, rows)
        pick = selection(hit, earlier)
        got = lax.dot_general(
            hit.astype(BF16), pick, (((1,), (1,)), ((), ())), preferred_element_type=F32
        )
        far[d] = jnp.where(spread(got) > 0.5, 0.0, MASKED)
        return 0

    lax.fori_loop(1, me + 1, gauge, 0)

    if relayed:

        @pl.when(relay_here)
        def _():
            for i in range(pairs):
                for kind in range(2):
                    root_copy(kind, i, me).wait_recv()
                    root_copy(kind, i, devices - 1, True).start()

    def arrived(kind, i, d):
        each(row_copy(kind, i, d, me, me - d), lambda c: c.wait_recv())

        @pl.when((d == me) & jnp.logical_not(relay_here))
        def _():
            root_copy(kind, i, d).wait_recv()

    own_start = core * head_width
    peer_start = other * head_width

    def att_copy(i):
        return pltpu.make_async_remote_copy(
            src_ref=att_own.at[i], dst_ref=att_peer.at[i], send_sem=att_sem.at[0, i],
            recv_sem=att_sem.at[1, i], device_id={"tp": other}, device_id_type=MESH,
        )

    def project(i):
        att_copy(i).wait_recv()
        both = jnp.concatenate([att_own[i], att_peer[i]], axis=1)
        weight = jnp.concatenate(
            [
                wo[pl.ds(pl.multiple_of(start + i * LANES, LANES), LANES), :]
                for start in (own_start, peer_start)
            ],
            axis=0,
        )
        return jnp.dot(both, weight, preferred_element_type=F32)

    wo_load.wait()
    for i in range(pairs):

        def attend(step, _):
            d = jnp.where(step == 1, me, step - 1)
            arrived(0, i, d)
            bias = far[d]
            bias = jnp.concatenate([bias, bias], axis=0)
            scores = scores_of(i, k_rows[d, i]) + bias
            old = peak[i]
            top = jnp.maximum(old, jnp.max(scores, axis=1, keepdims=True))
            factor = jnp.exp(old - top)
            weights = jnp.exp(scores - top[:, :picked])
            peak[i] = top
            total[i] = total[i] * factor
            total[i, :, :picked] += weights
            arrived(1, i, d)
            summed[i] = summed[i] * factor + jnp.dot(
                weights.astype(BF16), v_rows[d, i], preferred_element_type=F32
            )
            return 0

        lax.fori_loop(1, me + 1, attend, 0)
        ratio = summed[i] / jnp.sum(total[i], axis=1, keepdims=True)
        att_own[i] = jnp.where(lane < HEAD_DIM, ratio[:rows], ratio[rows:]).astype(BF16)
        att_copy(i).start()
        if i == 1:
            mixed[...] = project(0)
        elif i > 1:
            mixed[...] += project(i - 1)
    last = project(pairs - 1)
    if pairs > 1:
        last = mixed[...] + last
    out_ref[...] = last.astype(BF16)

    for i in range(pairs):
        att_copy(i).wait_send()
    tok_copy.wait_send()

    def drain_list(d, _):
        list_copy(d, me - d).wait_send()
        return 0

    lax.fori_loop(1, me + 1, drain_list, 0)

    def drain_rows(d, _):
        for i in range(pairs):
            each(row_copy(0, i, d, me + d, me), lambda c: c.wait_send())
            each(row_copy(1, i, d, me + d, me), lambda c: c.wait_send())
        return 0

    lax.fori_loop(1, devices - me, drain_rows, 0)

    @pl.when(me == 0)
    def _():
        def drain_root(d, _):
            for i in range(pairs):
                root_copy(0, i, d).wait_send()
                root_copy(1, i, d).wait_send()
            return 0

        lax.fori_loop(1, direct + 1, drain_root, 0)

    if relayed:

        @pl.when(relay_here)
        def _():
            for i in range(pairs):
                for kind in range(2):
                    root_copy(kind, i, devices - 1, True).wait_send()


def on_device(devices, tokens, query_weight, key_weight, value_weight, out_weight, chosen):
    rows, half = tokens.shape
    width, head_width = query_weight.shape
    pairs = head_width // LANES
    picked = CAP * BLOCK
    row_table, base_table = rotary_tables(rows, devices)
    vmem = pl.BlockSpec(memory_space=pltpu.VMEM)
    anywhere = pl.BlockSpec(memory_space=pl.ANY)
    dma = pltpu.SemaphoreType.DMA
    return pl.pallas_call(
        functools.partial(layer, devices),
        out_shape=pltpu.VMEM((rows, out_weight.shape[1]), BF16),
        in_specs=[anywhere] * 8,
        out_specs=vmem,
        scratch_shapes=[
            pltpu.VMEM(chosen.shape, jnp.int32),
            pltpu.VMEM(base_table.shape, F32),
            pltpu.VMEM((rows, 2 * LANES), F32),
            pltpu.VMEM((rows, half), BF16),
            pltpu.VMEM((rows, half), BF16),
            pltpu.VMEM((width, head_width), BF16),
            pltpu.VMEM((width, head_width), BF16),
            pltpu.VMEM((width, head_width), BF16),
            pltpu.VMEM(out_weight.shape, BF16),
            pltpu.VMEM((rows, head_width), F32),
            pltpu.VMEM((rows, head_width), F32),
            pltpu.VMEM((rows, head_width), F32),
            pltpu.VMEM((rows, head_width), BF16),
            pltpu.VMEM((rows, head_width), BF16),
            pltpu.VMEM((pairs, 2 * rows, LANES), BF16),
            pltpu.VMEM((devices,) + chosen.shape, jnp.int32),
            pltpu.VMEM((devices, picked, rows), BF16),
            pltpu.VMEM((devices, pairs, picked, LANES), BF16),
            pltpu.VMEM((devices, pairs, picked, LANES), BF16),
            pltpu.VMEM((devices, rows, picked), F32),
            pltpu.VMEM((pairs, 2 * rows, LANES), F32),
            pltpu.VMEM((pairs, 2 * rows, LANES), F32),
            pltpu.VMEM((pairs, 2 * rows, LANES), F32),
            pltpu.VMEM((rows, out_weight.shape[1]), F32),
            pltpu.VMEM((pairs, rows, LANES), BF16),
            pltpu.VMEM((pairs, rows, LANES), BF16),
            dma((8,)),
            dma((2,)),
            dma((2, pairs)),
            dma((devices,)),
            dma((devices,)),
            dma((2, pairs, devices)),
            dma((2, pairs, devices)),
            dma((2, pairs, devices)),
            dma((2, pairs)),
            dma((2, pairs)),
        ],
        compiler_params=pltpu.CompilerParams(
            collective_id=0, has_side_effects=True, vmem_limit_bytes=62 * 1024 * 1024
        ),
        name="layer",
    )(
        chosen, jnp.asarray(base_table), jnp.asarray(row_table), tokens,
        query_weight, key_weight, value_weight, out_weight,
    )


def solution(mesh):
    placed = (
        P(("dp", "kv"), "tp"),
        P(None, "tp"),
        P(None, "tp"),
        P(None, "tp"),
        P(None, "tp"),
        P(("dp", "kv"), None),
    )
    return jax.shard_map(
        functools.partial(on_device, mesh.shape["kv"]),
        mesh=mesh, in_specs=placed, out_specs=P(("dp", "kv"), "tp"), check_vma=False,
    )
```

time: 26.8 us -> 27.9 us (1.041)
  the two profiles are of different devices: /device:TPU:17 before, /device:TPU:25 now
where the time goes in v1:
time: 27.9 us; the launch traced here: 27.7 us
  Pallas kernels  26.9 us (96%)
  local copies, waits for them, and re-layouts  0.8 us (3%)
    pallas_call x1, Pallas kernels, on_device(): pl.pallas_call(functools.partial(layer, devices), out_shape=pltpu.VMEM((r...  26.9 us
    unnamed x1, local copies, waits for them, and re-layouts  0.8 us

profile of v1, /device:TPU:25, one launch (start us, length us, event | category | flops | bytes accessed | tf_op | source)
XLA Modules:
  0.0 27.7 jit_solution(13745871420717698163)
XLA Ops:
  0.0 26.9 %layer.1 = bf16[256,1024]{1,0:T(8,128)(2,1)S(1)} custom-call(s32[8,16]{1,0:T(8,128)} %chosen_hbm.1, f32[4,256]{1,0:T(4,128)} %constant.4.clone.base_hbm, f32[256,256]{1,0:T(8,128)} %constant.5.clone.row_hbm, bf16[256,1024]{1,0:T(8,128)(2,1)} %tok_hbm.1, bf16[2048,512]{1,0:T(8,128)(2,1)} %wq_hbm.1, bf16[2048,512]{1,0:T(8,128)(2,1)} %wk_hbm.1, ...), custom_call_target="tpu_custom_call" | custom-call | tf_op jit(solution)/shard_map/layer/pallas_call | solution.py:389
  26.9 0.8 %copy.10 = bf16[256,1024]{1,0:T(8,128)(2,1)} copy(bf16[256,1024]{1,0:T(8,128)(2,1)S(1)} %layer.1) | data formatting | bytes 1048576

commit v2 on v0

--- a/solution.py
+++ b/solution.py
@@ -38,11 +38,11 @@
     return hit
 
 
-def selection(hit, earlier):
+def selection(hit, earlier, slots=CAP * BLOCK):
     blocks, rows = hit.shape
     need = jnp.broadcast_to(jnp.max(hit, axis=0, keepdims=True), hit.shape)
     rank = jnp.dot(need.astype(BF16), earlier, preferred_element_type=F32)
-    shape = (CAP * BLOCK, rows)
+    shape = (slots, rows)
     slot_row = lax.broadcasted_iota(jnp.int32, shape, 0)
     column = lax.broadcasted_iota(jnp.int32, shape, 1)
     wanted = (slot_row // BLOCK).astype(F32)
@@ -363,11 +363,385 @@
                 root_copy(kind, devices - 1, True).wait_send()
 
 
+def short_layer(
+    devices,
+    chosen_hbm, tab_hbm, tok_hbm, wq_hbm, wk_hbm, wv_hbm, wo_hbm,
+    out_ref,
+    chosen_ref, tab, tok_own, tok_peer, wq, wk, wv, wo, q_acc, k_acc, v_acc, k_own, v_own, q2,
+    lists, picks, k_rows, v_rows, far, peak, total, summed, mixed, att_own, att_peer,
+    load_sem, tok_send, tok_recv, att_send, att_recv, list_send, list_recv, key_send, key_recv, root_recv,
+):
+    me = lax.axis_index("kv")
+    core = lax.axis_index("tp")
+    rows, half = tok_own.shape
+    pairs = k_own.shape[0]
+    picked = CAP * BLOCK
+    other = 1 - core
+    relayed = devices > 2
+    direct = devices - 2 if relayed else devices - 1
+    span = 2 if pairs % 2 == 0 else 1
+    groups = [list(range(start, start + span)) for start in range(0, pairs, span)]
+    buffers = ((k_own, k_rows), (v_own, v_rows))
+
+    loads = [
+        pltpu.make_async_copy(src, dst, load_sem.at[i])
+        for i, (src, dst) in enumerate(
+            ((chosen_hbm, chosen_ref), (tok_hbm, tok_own), (wk_hbm, wk), (tab_hbm, tab), (wv_hbm, wv), (wq_hbm, wq), (wo_hbm, wo))
+        )
+    ]
+    for load in loads:
+        load.start()
+    chosen_load, tok_load, wk_load, tab_load, wv_load, wq_load, wo_load = loads
+
+    barrier = pltpu.get_barrier_semaphore()
+    pl.semaphore_signal(barrier, inc=1, device_id={"tp": other}, device_id_type=MESH)
+    for d in range(1, devices):
+        pl.semaphore_signal(
+            barrier, inc=1, device_id={"kv": lax.rem(me + d, devices)}, device_id_type=MESH
+        )
+
+    for _, buffer in buffers:
+        for slot in range(devices - 1):
+            empty = slice(slot * LANES + picked, (slot + 1) * LANES)
+            buffer[:, empty, :] = jnp.zeros((pairs, LANES - picked, LANES), BF16)
+
+    own_half = pl.ds(pl.multiple_of(core * half, half), half)
+    peer_half = pl.ds(pl.multiple_of(other * half, half), half)
+
+    def list_copy(d):
+        return pltpu.make_async_remote_copy(
+            src_ref=chosen_ref, dst_ref=lists.at[d - 1], send_sem=list_send.at[0],
+            recv_sem=list_recv.at[d - 1], device_id={"kv": jnp.maximum(me - d, 0)}, device_id_type=MESH,
+        )
+
+    chunks = tok_recv.shape[0]
+    chunk = rows // chunks
+
+    def tok_copy(c):
+        part = slice(c * chunk, (c + 1) * chunk)
+        return pltpu.make_async_remote_copy(
+            src_ref=tok_own.at[part], dst_ref=tok_peer.at[part], send_sem=tok_send.at[0],
+            recv_sem=tok_recv.at[c], device_id={"tp": other}, device_id_type=MESH,
+        )
+
+    chosen_load.wait()
+    tok_load.wait()
+    pl.semaphore_wait(barrier, devices)
+    for d in range(1, devices):
+        pl.when(me >= d)(lambda d=d: list_copy(d).start())
+    for c in range(chunks):
+        tok_copy(c).start()
+
+    wk_load.wait()
+    k_acc[...] = jnp.dot(tok_own[...], wk[own_half, :], preferred_element_type=F32)
+    wv_load.wait()
+    v_acc[...] = jnp.dot(tok_own[...], wv[own_half, :], preferred_element_type=F32)
+    wq_load.wait()
+    q_acc[...] = jnp.dot(tok_own[...], wq[own_half, :], preferred_element_type=F32)
+
+    tab_load.wait()
+    lane = lax.broadcasted_iota(jnp.int32, (rows, LANES), 1)
+    base = tab[pl.ds(rows + me, 1), :]
+    row_cos, row_sin = tab[:rows, :LANES], tab[:rows, LANES:]
+    base_cos, base_sin = base[:, :LANES], base[:, LANES:]
+    cosine = row_cos * base_cos - row_sin * base_sin
+    sine = row_sin * base_cos + row_cos * base_sin
+    sine = jnp.where((lane % HEAD_DIM) < HEAD_DIM // 2, -sine, sine)
+    tab[:rows, :LANES] = cosine
+    tab[:rows, LANES:] = sine
+
+    def rotated(x, part):
+        first = (lax.broadcasted_iota(jnp.int32, x.shape, 1) % HEAD_DIM) < HEAD_DIM // 2
+        swapped = jnp.where(
+            first,
+            pltpu.roll(x, LANES - HEAD_DIM // 2, axis=1),
+            pltpu.roll(x, HEAD_DIM // 2, axis=1),
+        )
+        return x * tab[part, :LANES] + swapped * tab[part, LANES:]
+
+    row_i = lax.broadcasted_iota(jnp.int32, (rows, rows), 0)
+    col_i = lax.broadcasted_iota(jnp.int32, (rows, rows), 1)
+    earlier = jnp.where((row_i % BLOCK == 0) & (row_i // BLOCK < col_i // BLOCK), 1.0, 0.0).astype(BF16)
+
+    def choose(d, target):
+        list_copy(d).wait_recv()
+        slot = slice((target - 1) * LANES, target * LANES)
+        picks[slot, :] = selection(listed_columns(lists[d - 1], me, rows), earlier, LANES)
+
+    for m in range(devices - 1):
+
+        @pl.when(me == m)
+        def _(m=m):
+            for d in range(1, devices - m):
+                choose(d, m + d)
+
+    def row_copy(kind, i, m, d):
+        buffer = buffers[kind][1]
+        low = BLOCK if m == 0 else 0
+        return pltpu.make_async_remote_copy(
+            src_ref=buffer.at[i, slice((m + d - 1) * LANES + low, (m + d - 1) * LANES + picked)],
+            dst_ref=buffer.at[i, slice((d - 1) * LANES + low, (d - 1) * LANES + picked)],
+            send_sem=key_send.at[kind], recv_sem=key_recv.at[kind, i],
+            device_id={"kv": m + d}, device_id_type=MESH,
+        )
+
+    def root_copy(kind, g, d, passing=False):
+        own, buffer = buffers[kind]
+        some = slice(groups[g][0], groups[g][-1] + 1)
+        here = lambda slot: buffer.at[some, slice((slot - 1) * LANES, (slot - 1) * LANES + BLOCK)]
+        return pltpu.make_async_remote_copy(
+            src_ref=here(devices - 2) if passing else own.at[some, slice(0, BLOCK)], dst_ref=here(d),
+            send_sem=key_send.at[kind], recv_sem=root_recv.at[kind, g],
+            device_id={"kv": d}, device_id_type=MESH,
+        )
+
+    def send(kind, g):
+        own, buffer = buffers[kind]
+        some = groups[g]
+
+        @pl.when(me == 0)
+        def _():
+            for d in range(direct, 0, -1):
+                root_copy(kind, g, d).start()
+
+        for m in range(devices - 1):
+
+            @pl.when(me == m)
+            def _(m=m):
+                wide = jnp.concatenate([own[i] for i in some], axis=1)
+                got = jnp.dot(picks[m * LANES :, :], wide, preferred_element_type=F32).astype(BF16)
+                for n, i in enumerate(some):
+                    buffer[i, m * LANES :, :] = got[:, n * LANES : (n + 1) * LANES]
+                for i in some:
+                    for d in range(1, devices - m):
+                        row_copy(kind, i, m, d).start()
+
+    for g, some in enumerate(groups):
+        columns = slice(some[0] * LANES, (some[-1] + 1) * LANES)
+        parts = [slice(c * chunk, (c + 1) * chunk) for c in range(chunks)] if g == 0 else [slice(0, rows)]
+        for c, part in enumerate(parts):
+            if g == 0:
+                tok_copy(c).wait_recv()
+            k_full = k_acc[part, columns] + jnp.dot(
+                tok_peer[part, :], wk[peer_half, columns], preferred_element_type=F32
+            )
+            for n, i in enumerate(some):
+                k_own[i, part, :] = rotated(k_full[:, n * LANES : (n + 1) * LANES], part).astype(BF16)
+        send(0, g)
+        v_full = v_acc[:, columns] + jnp.dot(tok_peer[...], wv[peer_half, columns], preferred_element_type=F32)
+        for n, i in enumerate(some):
+            v_own[i] = v_full[:, n * LANES : (n + 1) * LANES].astype(BF16)
+        send(1, g)
+
+    q_full = q_acc[...] + jnp.dot(tok_peer[...], wq[peer_half, :], preferred_element_type=F32)
+    for i in range(pairs):
+        tile = slice(i * LANES, (i + 1) * LANES)
+        q = rotated(q_full[:, tile], slice(0, rows)).astype(BF16).astype(F32) * (HEAD_DIM**-0.5)
+        q2[i, :rows, :] = jnp.where(lane < HEAD_DIM, q, 0.0).astype(BF16)
+        q2[i, rows:, :] = jnp.where(lane < HEAD_DIM, 0.0, q).astype(BF16)
+
+    chosen = chosen_ref[...]
+
+    def spread(hit):
+        keys = hit.shape[1]
+        blocks = hit.shape[0]
+        wide = jnp.broadcast_to(hit[:, None, :], (blocks, BLOCK, keys))
+        return wide.reshape(blocks * BLOCK, keys)
+
+    def scores_of(i, keys):
+        return lax.dot_general(
+            q2[i], keys, (((1,), (1,)), ((), ())), preferred_element_type=F32
+        )
+
+    def lane_sums(weights):
+        return sum(weights[:, j : j + LANES] for j in range(0, weights.shape[1], LANES))
+
+    listed = spread(listed_columns(chosen, me, rows))
+    bias = jnp.where((listed > 0.5) & (col_i <= row_i), 0.0, MASKED)
+    bias = jnp.concatenate([bias, bias], axis=0)
+    for i in range(pairs):
+        scores = scores_of(i, k_own[i]) + bias
+        top = jnp.max(scores, axis=1, keepdims=True)
+        weights = jnp.exp(scores - top)
+        peak[i] = jnp.broadcast_to(top, peak.shape[1:])
+        total[i] = lane_sums(weights)
+        summed[i] = jnp.dot(weights.astype(BF16), v_own[i], preferred_element_type=F32)
+
+    for d in range(1, devices):
+
+        @pl.when(me >= d)
+        def _(d=d):
+            hit = listed_columns(chosen, me - d, rows)
+            pick = selection(hit, earlier, LANES)
+            got = lax.dot_general(
+                hit.astype(BF16), pick, (((1,), (1,)), ((), ())), preferred_element_type=F32
+            )
+            far[:, (d - 1) * LANES : d * LANES] = jnp.where(spread(got) > 0.5, 0.0, MASKED)
+
+    def att_copy(i):
+        return pltpu.make_async_remote_copy(
+            src_ref=att_own.at[i], dst_ref=att_peer.at[i], send_sem=att_send.at[0],
+            recv_sem=att_recv.at[i], device_id={"tp": other}, device_id_type=MESH,
+        )
+
+    def finish(i, result):
+        att_own[i] = jnp.where(lane < HEAD_DIM, result[:rows], result[rows:]).astype(BF16)
+        att_copy(i).start()
+
+    def project(i):
+        att_copy(i).wait_recv()
+        both = jnp.concatenate([att_own[i], att_peer[i]], axis=1)
+        weight = jnp.concatenate(
+            [
+                wo[pl.ds(pl.multiple_of((device * pairs + i) * LANES, LANES), LANES), :]
+                for device in (core, other)
+            ],
+            axis=0,
+        )
+        return jnp.dot(both, weight, preferred_element_type=F32)
+
+    def arrived(kind, i, m):
+        buffer = buffers[kind][1]
+        space = buffer.at[i, slice(0, m * picked - BLOCK)]
+        pltpu.make_async_copy(space, space, key_recv.at[kind, i]).wait()
+
+    def pass_root(g):
+        for kind in range(2):
+            root_copy(kind, g, devices - 2).wait_recv()
+            root_copy(kind, g, devices - 1, True).start()
+
+    wo_load.wait()
+    for i in range(pairs):
+
+        @pl.when(me == 0)
+        def _(i=i):
+            finish(i, summed[i] / jnp.sum(total[i], axis=1, keepdims=True))
+
+        for m in range(1, devices):
+
+            @pl.when(me == m)
+            def _(i=i, m=m):
+                opens = [g for g, some in enumerate(groups) if some[0] == i]
+                passes = relayed and m == devices - 2
+                if passes:
+                    for g in range(len(groups)):
+                        if g == i:
+                            pass_root(g)
+                else:
+                    for g in opens:
+                        root_copy(0, g, m).wait_recv()
+                arrived(0, i, m)
+                keys = slice(0, m * LANES)
+                scores = scores_of(i, k_rows[i, keys, :]) + jnp.concatenate([far[:, keys], far[:, keys]], axis=0)
+                old = peak[i]
+                top = jnp.maximum(old, jnp.max(scores, axis=1, keepdims=True))
+                factor = jnp.exp(old - top)
+                weights = jnp.exp(scores - jnp.concatenate([top] * m, axis=1))
+                inverse = 1.0 / jnp.sum(total[i] * factor + lane_sums(weights), axis=1, keepdims=True)
+                before = summed[i] * (factor * inverse)
+                weights = weights.astype(BF16)
+                if not passes:
+                    for g in opens:
+                        root_copy(1, g, m).wait_recv()
+                arrived(1, i, m)
+                after = jnp.dot(weights, v_rows[i, keys, :], preferred_element_type=F32)
+                finish(i, before + after * inverse)
+
+        if i == 1:
+            mixed[...] = project(0)
+        elif i > 1:
+            mixed[...] += project(i - 1)
+    last = project(pairs - 1)
+    if pairs > 1:
+        last = mixed[...] + last
+    out_ref[...] = last.astype(BF16)
+
+    pltpu.make_async_copy(att_own, att_own, att_send.at[0]).wait()
+    pltpu.make_async_copy(tok_own, tok_own, tok_send.at[0]).wait()
+    for m in range(devices):
+
+        @pl.when(me == m)
+        def _(m=m):
+            if m > 0:
+                space = lists.at[slice(0, m)]
+                pltpu.make_async_copy(space, space, list_send.at[0]).wait()
+            sent = (devices - 1 - m) * (picked if m else picked - BLOCK)
+            if m == 0:
+                sent += direct * BLOCK
+            elif relayed and m == devices - 2:
+                sent += BLOCK
+            if sent:
+                for kind in range(2):
+                    space = buffers[kind][1].at[:, slice(0, sent)]
+                    pltpu.make_async_copy(space, space, key_send.at[kind]).wait()
+
+
+def short_call(devices, tokens, query_weight, key_weight, value_weight, out_weight, chosen):
+    rows, half = tokens.shape
+    width, head_width = query_weight.shape
+    pairs = head_width // LANES
+    table = np.concatenate(rotary_tables(rows, devices), axis=0)
+    vmem = pl.BlockSpec(memory_space=pltpu.VMEM)
+    anywhere = pl.BlockSpec(memory_space=pl.ANY)
+    dma = pltpu.SemaphoreType.DMA
+    groups = pairs // 2 if pairs % 2 == 0 else pairs
+    others = devices - 1
+    return pl.pallas_call(
+        functools.partial(short_layer, devices),
+        out_shape=pltpu.VMEM((rows, out_weight.shape[1]), BF16),
+        in_specs=[anywhere] * 7,
+        out_specs=vmem,
+        scratch_shapes=[
+            pltpu.VMEM(chosen.shape, jnp.int32),
+            pltpu.VMEM(table.shape, F32),
+            pltpu.VMEM((rows, half), BF16),
+            pltpu.VMEM((rows, half), BF16),
+            pltpu.VMEM((width, head_width), BF16),
+            pltpu.VMEM((width, head_width), BF16),
+            pltpu.VMEM((width, head_width), BF16),
+            pltpu.VMEM(out_weight.shape, BF16),
+            pltpu.VMEM((rows, head_width), F32),
+            pltpu.VMEM((rows, head_width), F32),
+            pltpu.VMEM((rows, head_width), F32),
+            pltpu.VMEM((pairs, rows, LANES), BF16),
+            pltpu.VMEM((pairs, rows, LANES), BF16),
+            pltpu.VMEM((pairs, 2 * rows, LANES), BF16),
+            pltpu.VMEM((others,) + chosen.shape, jnp.int32),
+            pltpu.VMEM((others * LANES, rows), BF16),
+            pltpu.VMEM((pairs, others * LANES, LANES), BF16),
+            pltpu.VMEM((pairs, others * LANES, LANES), BF16),
+            pltpu.VMEM((rows, others * LANES), F32),
+            pltpu.VMEM((pairs, 2 * rows, LANES), F32),
+            pltpu.VMEM((pairs, 2 * rows, LANES), F32),
+            pltpu.VMEM((pairs, 2 * rows, LANES), F32),
+            pltpu.VMEM((rows, out_weight.shape[1]), F32),
+            pltpu.VMEM((pairs, rows, LANES), BF16),
+            pltpu.VMEM((pairs, rows, LANES), BF16),
+            dma((7,)),
+            dma((1,)),
+            dma((2,)),
+            dma((1,)),
+            dma((pairs,)),
+            dma((1,)),
+            dma((others,)),
+            dma((2,)),
+            dma((2, pairs)),
+            dma((2, groups)),
+        ],
+        compiler_params=pltpu.CompilerParams(
+            collective_id=0, has_side_effects=True, vmem_limit_bytes=62 * 1024 * 1024
+        ),
+        name="layer",
+    )(chosen, jnp.asarray(table), tokens, query_weight, key_weight, value_weight, out_weight)
+
+
 def on_device(devices, tokens, query_weight, key_weight, value_weight, out_weight, chosen):
     rows, half = tokens.shape
     width, head_width = query_weight.shape
     pairs = head_width // LANES
     picked = CAP * BLOCK
+    if devices <= 4:
+        return short_call(devices, tokens, query_weight, key_weight, value_weight, out_weight, chosen)
     row_table, base_table = rotary_tables(rows, devices)
     vmem = pl.BlockSpec(memory_space=pltpu.VMEM)
     anywhere = pl.BlockSpec(memory_space=pl.ANY)

time: 26.8 us -> 26 us (0.970)
  the two profiles are of different devices: /device:TPU:17 before, /device:TPU:25 now
where the time goes in v2:
time: 26 us; the launch traced here: 25.9 us
  Pallas kernels  25.1 us (97%)
  local copies, waits for them, and re-layouts  0.8 us (3%)
    pallas_call x1, Pallas kernels, short_call(): pl.pallas_call(functools.partial(short_layer, devices), out_shape=pltpu.V...  25.1 us
    unnamed x1, local copies, waits for them, and re-layouts  0.8 us

profile of v2, /device:TPU:25, one launch (start us, length us, event | category | flops | bytes accessed | tf_op | source)
XLA Modules:
  0.0 25.9 jit_solution(11017849720720675835)
XLA Ops:
  0.0 25.1 %layer.1 = bf16[256,1024]{1,0:T(8,128)(2,1)S(1)} custom-call(s32[8,16]{1,0:T(8,128)} %chosen_hbm.1, f32[260,256]{1,0:T(8,128)} %constant.2.clone.tab_hbm, bf16[256,1024]{1,0:T(8,128)(2,1)} %tok_hbm.1, bf16[2048,512]{1,0:T(8,128)(2,1)} %wq_hbm.1, bf16[2048,512]{1,0:T(8,128)(2,1)} %wk_hbm.1, bf16[2048,512]{1,0:T(8,128)(2,1)} %wv_hbm.1, bf16[1024,1024]{1,0:T(8,128)(2,1)} %wo_hbm.1), custom_call_target="tpu_custom_call" | custom-call | tf_op jit(solution)/shard_map/layer/pallas_call | solution.py:689
  25.1 0.8 %copy.9 = bf16[256,1024]{1,0:T(8,128)(2,1)} copy(bf16[256,1024]{1,0:T(8,128)(2,1)S(1)} %layer.1) | data formatting | bytes 1048576

commit v3 on v2

--- a/solution.py
+++ b/solution.py
@@ -368,8 +368,8 @@
     chosen_hbm, tab_hbm, tok_hbm, wq_hbm, wk_hbm, wv_hbm, wo_hbm,
     out_ref,
     chosen_ref, tab, tok_own, tok_peer, wq, wk, wv, wo, q_acc, k_acc, v_acc, k_own, v_own, q2,
-    lists, picks, k_rows, v_rows, far, peak, total, summed, mixed, att_own, att_peer,
-    load_sem, tok_send, tok_recv, att_send, att_recv, list_send, list_recv, key_send, key_recv, root_recv,
+    lists, picks, k_rows, v_rows, far, peak, total, summed, weigh, mixed, att_own, att_peer, seed,
+    load_sem, tok_send, tok_recv, att_send, att_recv, list_send, list_recv, key_send, key_recv, root_recv, seed_send, seed_recv, seed_ready,
 ):
     me = lax.axis_index("kv")
     core = lax.axis_index("tp")
@@ -377,8 +377,6 @@
     pairs = k_own.shape[0]
     picked = CAP * BLOCK
     other = 1 - core
-    relayed = devices > 2
-    direct = devices - 2 if relayed else devices - 1
     span = 2 if pairs % 2 == 0 else 1
     groups = [list(range(start, start + span)) for start in range(0, pairs, span)]
     buffers = ((k_own, k_rows), (v_own, v_rows))
@@ -395,10 +393,12 @@
 
     barrier = pltpu.get_barrier_semaphore()
     pl.semaphore_signal(barrier, inc=1, device_id={"tp": other}, device_id_type=MESH)
-    for d in range(1, devices):
-        pl.semaphore_signal(
-            barrier, inc=1, device_id={"kv": lax.rem(me + d, devices)}, device_id_type=MESH
-        )
+
+    def greet(d, _):
+        pl.semaphore_signal(barrier, inc=1, device_id={"kv": d}, device_id_type=MESH)
+        return 0
+
+    lax.fori_loop(me + 1, devices, greet, 0)
 
     for _, buffer in buffers:
         for slot in range(devices - 1):
@@ -425,12 +425,31 @@
         )
 
     chosen_load.wait()
-    tok_load.wait()
-    pl.semaphore_wait(barrier, devices)
+    pl.semaphore_wait(barrier, 1 + me)
     for d in range(1, devices):
         pl.when(me >= d)(lambda d=d: list_copy(d).start())
+    if devices > 2:
+
+        @pl.when(me == 2)
+        def _():
+            pl.semaphore_signal(seed_ready, inc=1, device_id={"kv": 0}, device_id_type=MESH)
+
+    tok_load.wait()
     for c in range(chunks):
         tok_copy(c).start()
+
+    def seed_copy(source, target):
+        return pltpu.make_async_remote_copy(
+            src_ref=seed.at[0] if source else tok_own.at[slice(0, BLOCK)], dst_ref=seed.at[0],
+            send_sem=seed_send.at[0], recv_sem=seed_recv.at[0],
+            device_id={"kv": target}, device_id_type=MESH,
+        )
+
+    def seed_share():
+        return pltpu.make_async_remote_copy(
+            src_ref=seed.at[0], dst_ref=seed.at[1], send_sem=seed_send.at[1], recv_sem=seed_recv.at[1],
+            device_id={"tp": other}, device_id_type=MESH,
+        )
 
     wk_load.wait()
     k_acc[...] = jnp.dot(tok_own[...], wk[own_half, :], preferred_element_type=F32)
@@ -439,9 +458,16 @@
     wq_load.wait()
     q_acc[...] = jnp.dot(tok_own[...], wq[own_half, :], preferred_element_type=F32)
 
+    if devices > 2:
+
+        @pl.when(me == 0)
+        def _():
+            pl.semaphore_wait(seed_ready, 1)
+            seed_copy(0, 2).start()
+
     tab_load.wait()
     lane = lax.broadcasted_iota(jnp.int32, (rows, LANES), 1)
-    base = tab[pl.ds(rows + me, 1), :]
+    base = tab[pl.ds(rows + BLOCK + me, 1), :]
     row_cos, row_sin = tab[:rows, :LANES], tab[:rows, LANES:]
     base_cos, base_sin = base[:, :LANES], base[:, LANES:]
     cosine = row_cos * base_cos - row_sin * base_sin
@@ -467,13 +493,6 @@
         list_copy(d).wait_recv()
         slot = slice((target - 1) * LANES, target * LANES)
         picks[slot, :] = selection(listed_columns(lists[d - 1], me, rows), earlier, LANES)
-
-    for m in range(devices - 1):
-
-        @pl.when(me == m)
-        def _(m=m):
-            for d in range(1, devices - m):
-                choose(d, m + d)
 
     def row_copy(kind, i, m, d):
         buffer = buffers[kind][1]
@@ -485,36 +504,44 @@
             device_id={"kv": m + d}, device_id_type=MESH,
         )
 
-    def root_copy(kind, g, d, passing=False):
+    def root_copy(kind, g):
         own, buffer = buffers[kind]
         some = slice(groups[g][0], groups[g][-1] + 1)
-        here = lambda slot: buffer.at[some, slice((slot - 1) * LANES, (slot - 1) * LANES + BLOCK)]
         return pltpu.make_async_remote_copy(
-            src_ref=here(devices - 2) if passing else own.at[some, slice(0, BLOCK)], dst_ref=here(d),
+            src_ref=own.at[some, slice(0, BLOCK)], dst_ref=buffer.at[some, slice(0, BLOCK)],
             send_sem=key_send.at[kind], recv_sem=root_recv.at[kind, g],
-            device_id={"kv": d}, device_id_type=MESH,
+            device_id={"kv": 1}, device_id_type=MESH,
         )
 
     def send(kind, g):
         own, buffer = buffers[kind]
         some = groups[g]
 
-        @pl.when(me == 0)
-        def _():
-            for d in range(direct, 0, -1):
-                root_copy(kind, g, d).start()
+        def gather(low, high):
+            wide = jnp.concatenate([own[i] for i in some], axis=1)
+            span = slice((low - 1) * LANES, high * LANES)
+            got = jnp.dot(picks[span, :], wide, preferred_element_type=F32).astype(BF16)
+            for n, i in enumerate(some):
+                buffer[i, span, :] = got[:, n * LANES : (n + 1) * LANES]
 
         for m in range(devices - 1):
 
             @pl.when(me == m)
             def _(m=m):
-                wide = jnp.concatenate([own[i] for i in some], axis=1)
-                got = jnp.dot(picks[m * LANES :, :], wide, preferred_element_type=F32).astype(BF16)
-                for n, i in enumerate(some):
-                    buffer[i, m * LANES :, :] = got[:, n * LANES : (n + 1) * LANES]
-                for i in some:
-                    for d in range(1, devices - m):
-                        row_copy(kind, i, m, d).start()
+                targets = list(range(m + 1, devices))
+                if kind == 0 and g == 0:
+                    for t in targets:
+                        choose(t - m, t)
+                        gather(t, t)
+                        for i in some:
+                            row_copy(kind, i, m, t - m).start()
+                else:
+                    gather(m + 1, devices - 1)
+                    for i in some:
+                        for t in targets[1:] + targets[:1] if m == 0 else targets:
+                            row_copy(kind, i, m, t - m).start()
+                if m == 0:
+                    root_copy(kind, g).start()
 
     for g, some in enumerate(groups):
         columns = slice(some[0] * LANES, (some[-1] + 1) * LANES)
@@ -527,6 +554,14 @@
             )
             for n, i in enumerate(some):
                 k_own[i, part, :] = rotated(k_full[:, n * LANES : (n + 1) * LANES], part).astype(BF16)
+        if g == min(1, len(groups) - 1) and devices > 3:
+
+            @pl.when(me == 2)
+            def _():
+                seed_copy(2, 2).wait_recv()
+                seed_copy(2, 3).start()
+                seed_share().start()
+
         send(0, g)
         v_full = v_acc[:, columns] + jnp.dot(tok_peer[...], wv[peer_half, columns], preferred_element_type=F32)
         for n, i in enumerate(some):
@@ -567,6 +602,13 @@
         total[i] = lane_sums(weights)
         summed[i] = jnp.dot(weights.astype(BF16), v_own[i], preferred_element_type=F32)
 
+    if devices > 2:
+
+        @pl.when(me == devices - 1)
+        def _():
+            seed_copy(2, devices - 1).wait_recv()
+            seed_share().start()
+
     for d in range(1, devices):
 
         @pl.when(me >= d)
@@ -605,52 +647,86 @@
         space = buffer.at[i, slice(0, m * picked - BLOCK)]
         pltpu.make_async_copy(space, space, key_recv.at[kind, i]).wait()
 
-    def pass_root(g):
-        for kind in range(2):
-            root_copy(kind, g, devices - 2).wait_recv()
-            root_copy(kind, g, devices - 1, True).start()
+    if devices > 2:
+
+        @pl.when(me >= 2)
+        def _():
+            seed_share().wait_recv()
+            table = tab[rows : rows + BLOCK, :]
+            first = (lax.broadcasted_iota(jnp.int32, (BLOCK, LANES), 1) % HEAD_DIM) < HEAD_DIM // 2
+            block_cos = table[:, :LANES]
+            block_sin = jnp.where(first, -table[:, LANES:], table[:, LANES:])
+            for kind, weight in enumerate((wk, wv)):
+                grown = jnp.dot(seed[0], weight[own_half, :], preferred_element_type=F32)
+                grown = grown + jnp.dot(seed[1], weight[peer_half, :], preferred_element_type=F32)
+                at = pl.ds(pl.multiple_of((me - 1) * LANES, LANES), BLOCK)
+                for i in range(pairs):
+                    x = grown[:, i * LANES : (i + 1) * LANES]
+                    if kind == 0:
+                        swapped = jnp.where(
+                            first,
+                            pltpu.roll(x, LANES - HEAD_DIM // 2, axis=1),
+                            pltpu.roll(x, HEAD_DIM // 2, axis=1),
+                        )
+                        x = x * block_cos + swapped * block_sin
+                    buffers[kind][1][i, at, :] = x.astype(BF16)
+
+    def key_part(m, i, n):
+        arrived(0, i, m)
+        keys = slice(0, m * LANES)
+        scores = scores_of(i, k_rows[i, keys, :]) + jnp.concatenate([far[:, keys], far[:, keys]], axis=0)
+        old = peak[i]
+        top = jnp.maximum(old, jnp.max(scores, axis=1, keepdims=True))
+        factor = jnp.exp(old - top)
+        weights = jnp.exp(scores - jnp.concatenate([top] * m, axis=1))
+        inverse = 1.0 / jnp.sum(total[i] * factor + lane_sums(weights), axis=1, keepdims=True)
+        summed[i] = summed[i] * (factor * inverse)
+        total[i] = jnp.broadcast_to(inverse, total.shape[1:])
+        weigh[n, :, keys] = weights.astype(BF16)
+
+    def value_part(m, i, n):
+        arrived(1, i, m)
+        keys = slice(0, m * LANES)
+        after = jnp.dot(weigh[n, :, keys], v_rows[i, keys, :], preferred_element_type=F32)
+        finish(i, summed[i] + after * total[i])
 
     wo_load.wait()
-    for i in range(pairs):
+    for g, some in enumerate(groups):
+        for m in range(1, devices):
+
+            @pl.when(me == m)
+            def _(m=m, g=g, some=some):
+                if m == 1:
+                    root_copy(0, g).wait_recv()
+                for n, i in enumerate(some):
+                    key_part(m, i, n)
+
+        if g > 0:
+            for i in groups[g - 1]:
+                if i == 0:
+                    mixed[...] = project(i)
+                else:
+                    mixed[...] += project(i)
 
         @pl.when(me == 0)
-        def _(i=i):
-            finish(i, summed[i] / jnp.sum(total[i], axis=1, keepdims=True))
+        def _(some=some):
+            for i in some:
+                finish(i, summed[i] / jnp.sum(total[i], axis=1, keepdims=True))
 
         for m in range(1, devices):
 
             @pl.when(me == m)
-            def _(i=i, m=m):
-                opens = [g for g, some in enumerate(groups) if some[0] == i]
-                passes = relayed and m == devices - 2
-                if passes:
-                    for g in range(len(groups)):
-                        if g == i:
-                            pass_root(g)
-                else:
-                    for g in opens:
-                        root_copy(0, g, m).wait_recv()
-                arrived(0, i, m)
-                keys = slice(0, m * LANES)
-                scores = scores_of(i, k_rows[i, keys, :]) + jnp.concatenate([far[:, keys], far[:, keys]], axis=0)
-                old = peak[i]
-                top = jnp.maximum(old, jnp.max(scores, axis=1, keepdims=True))
-                factor = jnp.exp(old - top)
-                weights = jnp.exp(scores - jnp.concatenate([top] * m, axis=1))
-                inverse = 1.0 / jnp.sum(total[i] * factor + lane_sums(weights), axis=1, keepdims=True)
-                before = summed[i] * (factor * inverse)
-                weights = weights.astype(BF16)
-                if not passes:
-                    for g in opens:
-                        root_copy(1, g, m).wait_recv()
-                arrived(1, i, m)
-                after = jnp.dot(weights, v_rows[i, keys, :], preferred_element_type=F32)
-                finish(i, before + after * inverse)
-
-        if i == 1:
-            mixed[...] = project(0)
-        elif i > 1:
-            mixed[...] += project(i - 1)
+            def _(m=m, g=g, some=some):
+                if m == 1:
+                    root_copy(1, g).wait_recv()
+                for n, i in enumerate(some):
+                    value_part(m, i, n)
+
+    for i in groups[-1][:-1]:
+        if i == 0:
+            mixed[...] = project(i)
+        else:
+            mixed[...] += project(i)
     last = project(pairs - 1)
     if pairs > 1:
         last = mixed[...] + last
@@ -667,9 +743,11 @@
                 pltpu.make_async_copy(space, space, list_send.at[0]).wait()
             sent = (devices - 1 - m) * (picked if m else picked - BLOCK)
             if m == 0:
-                sent += direct * BLOCK
-            elif relayed and m == devices - 2:
                 sent += BLOCK
+            if devices > 2 and (m == 0 or 2 <= m < devices - 1):
+                pltpu.make_async_copy(seed.at[0], seed.at[0], seed_send.at[0]).wait()
+            if m >= 2:
+                pltpu.make_async_copy(seed.at[0], seed.at[0], seed_send.at[1]).wait()
             if sent:
                 for kind in range(2):
                     space = buffers[kind][1].at[:, slice(0, sent)]
@@ -680,7 +758,8 @@
     rows, half = tokens.shape
     width, head_width = query_weight.shape
     pairs = head_width // LANES
-    table = np.concatenate(rotary_tables(rows, devices), axis=0)
+    row_table, base_table = rotary_tables(rows, devices)
+    table = np.concatenate([row_table, row_table[:BLOCK], base_table], axis=0)
     vmem = pl.BlockSpec(memory_space=pltpu.VMEM)
     anywhere = pl.BlockSpec(memory_space=pl.ANY)
     dma = pltpu.SemaphoreType.DMA
@@ -714,12 +793,14 @@
             pltpu.VMEM((pairs, 2 * rows, LANES), F32),
             pltpu.VMEM((pairs, 2 * rows, LANES), F32),
             pltpu.VMEM((pairs, 2 * rows, LANES), F32),
+            pltpu.VMEM((pairs // groups, 2 * rows, others * LANES), BF16),
             pltpu.VMEM((rows, out_weight.shape[1]), F32),
             pltpu.VMEM((pairs, rows, LANES), BF16),
             pltpu.VMEM((pairs, rows, LANES), BF16),
+            pltpu.VMEM((2, BLOCK, half), BF16),
             dma((7,)),
             dma((1,)),
-            dma((2,)),
+            dma((1,)),
             dma((1,)),
             dma((pairs,)),
             dma((1,)),
@@ -727,6 +808,9 @@
             dma((2,)),
             dma((2, pairs)),
             dma((2, groups)),
+            dma((2,)),
+            dma((2,)),
+            pltpu.SemaphoreType.REGULAR,
         ],
         compiler_params=pltpu.CompilerParams(
             collective_id=0, has_side_effects=True, vmem_limit_bytes=62 * 1024 * 1024

time: 26 us -> 23.5 us (0.904)
  Pallas kernels: 25.1 us -> 22.4 us
    pallas_call x1, Pallas kernels: 25.1 us -> 22.4 us  [short_call(): pl.pallas_call(functools.partial(short_layer, devices), out_shape=pltpu.V...]
where the time goes in v3:
time: 23.5 us; the launch traced here: 23.2 us
  Pallas kernels  22.4 us (95%)
  local copies, waits for them, and re-layouts  0.8 us (3%)
    pallas_call x1, Pallas kernels, short_call(): pl.pallas_call(functools.partial(short_layer, devices), out_shape=pltpu.V...  22.4 us
    unnamed x1, local copies, waits for them, and re-layouts  0.8 us

profile of v3, /device:TPU:25, one launch (start us, length us, event | category | flops | bytes accessed | tf_op | source)
XLA Modules:
  0.0 23.2 jit_solution(3620344510255083985)
XLA Ops:
  0.0 22.4 %layer.1 = bf16[256,1024]{1,0:T(8,128)(2,1)S(1)} custom-call(s32[8,16]{1,0:T(8,128)} %chosen_hbm.1, f32[292,256]{1,0:T(8,128)} %constant.2.clone.tab_hbm, bf16[256,1024]{1,0:T(8,128)(2,1)} %tok_hbm.1, bf16[2048,512]{1,0:T(8,128)(2,1)} %wq_hbm.1, bf16[2048,512]{1,0:T(8,128)(2,1)} %wk_hbm.1, bf16[2048,512]{1,0:T(8,128)(2,1)} %wv_hbm.1, bf16[1024,1024]{1,0:T(8,128)(2,1)} %wo_hbm.1), custom_call_target="tpu_custom_call" | custom-call | tf_op jit(solution)/shard_map/layer/pallas_call | solution.py:768
  22.4 0.8 %copy.9 = bf16[256,1024]{1,0:T(8,128)(2,1)} copy(bf16[256,1024]{1,0:T(8,128)(2,1)S(1)} %layer.1) | data formatting | bytes 1048576

commit v4 on v0

--- a/solution.py
+++ b/solution.py
@@ -38,11 +38,11 @@
     return hit
 
 
-def selection(hit, earlier):
+def selection(hit, earlier, slots=CAP * BLOCK):
     blocks, rows = hit.shape
     need = jnp.broadcast_to(jnp.max(hit, axis=0, keepdims=True), hit.shape)
     rank = jnp.dot(need.astype(BF16), earlier, preferred_element_type=F32)
-    shape = (CAP * BLOCK, rows)
+    shape = (slots, rows)
     slot_row = lax.broadcasted_iota(jnp.int32, shape, 0)
     column = lax.broadcasted_iota(jnp.int32, shape, 1)
     wanted = (slot_row // BLOCK).astype(F32)
@@ -363,11 +363,650 @@
                 root_copy(kind, devices - 1, True).wait_send()
 
 
+def quad_layer(
+    chosen_hbm, tab_hbm, tok_hbm, wq_hbm, wk_hbm, wv_hbm, wo_hbm,
+    out_ref,
+    chosen_ref, tab, tok_own, tok_peer, wq, wk, wv, wo, q_acc, k_acc, v_acc, k_own, v_own, q2,
+    lists, picks, k_rows, v_rows, far, peak, total, summed, weigh, mixed, att_own, att_peer,
+    k_serve, v_serve, far_serve, q_out, q_in, state_out, state_in,
+    load_sem, tok_send, tok_recv, att_send, att_recv, list_send, list_recv, key_send, key_recv, root_recv,
+    wire_send, wire_recv,
+):
+    devices, server = 4, 1
+    me = lax.axis_index("kv")
+    core = lax.axis_index("tp")
+    rows, half = tok_own.shape
+    pairs = k_own.shape[0]
+    picked = CAP * BLOCK
+    other = 1 - core
+    served = list(range(pairs - q_out.shape[0], pairs))
+    plain = list(range(pairs - q_out.shape[0]))
+    clients = [2, 3]
+    buffers = ((k_own, k_rows), (v_own, v_rows))
+    serves = (k_serve, v_serve)
+
+    chosen_load, tok_load, tab_load, wk_load, wv_load, wq_load, wo_load = [
+        pltpu.make_async_copy(src, dst, load_sem.at[i])
+        for i, (src, dst) in enumerate(
+            ((chosen_hbm, chosen_ref), (tok_hbm, tok_own), (tab_hbm, tab), (wk_hbm, wk), (wv_hbm, wv), (wq_hbm, wq), (wo_hbm, wo))
+        )
+    ]
+    chosen_load.start()
+    tok_load.start()
+
+    @pl.when(me < 2)
+    def _():
+        for load in (wk_load, tab_load, wv_load, wq_load):
+            load.start()
+
+    @pl.when(me >= 2)
+    def _():
+        for load in (wq_load, tab_load, wk_load, wv_load):
+            load.start()
+
+    wo_load.start()
+
+    barrier = pltpu.get_barrier_semaphore()
+    pl.semaphore_signal(barrier, inc=1, device_id={"tp": other}, device_id_type=MESH)
+
+    def greet(d, _):
+        pl.semaphore_signal(barrier, inc=1, device_id={"kv": d}, device_id_type=MESH)
+        return 0
+
+    lax.fori_loop(me + 1, devices, greet, 0)
+
+    for _, buffer in buffers:
+        for slot in range(devices - 1):
+            empty = slice(slot * LANES + picked, (slot + 1) * LANES)
+            buffer[:, empty, :] = jnp.zeros((pairs, LANES - picked, LANES), BF16)
+    for buffer in serves:
+        shape = buffer.shape[:2] + (LANES - picked, LANES)
+        buffer[:, :, slice(picked, LANES), :] = jnp.zeros(shape, BF16)
+
+    own_half = pl.ds(pl.multiple_of(core * half, half), half)
+    peer_half = pl.ds(pl.multiple_of(other * half, half), half)
+
+    def list_copy(d):
+        return pltpu.make_async_remote_copy(
+            src_ref=chosen_ref, dst_ref=lists.at[d - 1], send_sem=list_send.at[0],
+            recv_sem=list_recv.at[d - 1], device_id={"kv": jnp.maximum(me - d, 0)}, device_id_type=MESH,
+        )
+
+    tok_copy = pltpu.make_async_remote_copy(
+        src_ref=tok_own, dst_ref=tok_peer, send_sem=tok_send.at[0],
+        recv_sem=tok_recv.at[0], device_id={"tp": other}, device_id_type=MESH,
+    )
+
+    chosen_load.wait()
+    pl.semaphore_wait(barrier, 1 + me)
+    for d in range(1, devices):
+        pl.when(me >= d)(lambda d=d: list_copy(d).start())
+    tok_load.wait()
+    tok_copy.start()
+
+    lane = lax.broadcasted_iota(jnp.int32, (rows, LANES), 1)
+    first = (lane % HEAD_DIM) < HEAD_DIM // 2
+    row_i = lax.broadcasted_iota(jnp.int32, (rows, rows), 0)
+    col_i = lax.broadcasted_iota(jnp.int32, (rows, rows), 1)
+    earlier = jnp.where((row_i % BLOCK == 0) & (row_i // BLOCK < col_i // BLOCK), 1.0, 0.0).astype(BF16)
+
+    def turn_tables():
+        tab_load.wait()
+        base = tab[pl.ds(rows + me, 1), :]
+        row_cos, row_sin = tab[:rows, :LANES], tab[:rows, LANES:]
+        base_cos, base_sin = base[:, :LANES], base[:, LANES:]
+        cosine = row_cos * base_cos - row_sin * base_sin
+        sine = row_sin * base_cos + row_cos * base_sin
+        tab[:rows, :LANES] = cosine
+        tab[:rows, LANES:] = jnp.where(first, -sine, sine)
+
+    def rotated(x):
+        swapped = jnp.where(
+            first,
+            pltpu.roll(x, LANES - HEAD_DIM // 2, axis=1),
+            pltpu.roll(x, HEAD_DIM // 2, axis=1),
+        )
+        return x * tab[:rows, :LANES] + swapped * tab[:rows, LANES:]
+
+    def begin(acc, weight):
+        acc[...] = jnp.dot(tok_own[...], weight[own_half, :], preferred_element_type=F32)
+
+    def rest(acc, weight, some):
+        columns = slice(some[0] * LANES, (some[-1] + 1) * LANES)
+        full = acc[:, columns] + jnp.dot(tok_peer[...], weight[peer_half, columns], preferred_element_type=F32)
+        return [full[:, n * LANES : (n + 1) * LANES] for n in range(len(some))]
+
+    def make_keys(some):
+        for i, x in zip(some, rest(k_acc, wk, some)):
+            k_own[i] = rotated(x).astype(BF16)
+
+    def make_values(some):
+        for i, x in zip(some, rest(v_acc, wv, some)):
+            v_own[i] = x.astype(BF16)
+
+    def make_queries(some, share=False):
+        for i, x in zip(some, rest(q_acc, wq, some)):
+            q = rotated(x).astype(BF16).astype(F32) * (HEAD_DIM**-0.5)
+            if share:
+                q_out[i - served[0]] = q.astype(BF16)
+            q2[i, :rows, :] = jnp.where(lane < HEAD_DIM, q, 0.0).astype(BF16)
+            q2[i, rows:, :] = jnp.where(lane < HEAD_DIM, 0.0, q).astype(BF16)
+
+    def choose(m, t):
+        list_copy(t - m).wait_recv()
+        slot = slice((t - 1) * LANES, t * LANES)
+        picks[slot, :] = selection(listed_columns(lists[t - m - 1], me, rows), earlier, LANES)
+
+    def gather(sources, low, high):
+        wide = jnp.concatenate([ref[i] for ref, i in sources], axis=1)
+        got = jnp.dot(
+            picks[(low - 1) * LANES : high * LANES, :], wide, preferred_element_type=F32
+        ).astype(BF16)
+        return [got[:, n * LANES : (n + 1) * LANES] for n in range(len(sources))]
+
+    def row_copy(kind, i, m, t):
+        buffer = buffers[kind][1]
+        low = BLOCK if m == 0 else 0
+        return pltpu.make_async_remote_copy(
+            src_ref=buffer.at[i, slice((t - 1) * LANES + low, (t - 1) * LANES + picked)],
+            dst_ref=buffer.at[i, slice((t - m - 1) * LANES + low, (t - m - 1) * LANES + picked)],
+            send_sem=key_send.at[kind], recv_sem=key_recv.at[kind, i],
+            device_id={"kv": t}, device_id_type=MESH,
+        )
+
+    def serve_copy(kind, i, c):
+        return pltpu.make_async_remote_copy(
+            src_ref=buffers[kind][1].at[i, slice((c - 1) * LANES + BLOCK, (c - 1) * LANES + picked)],
+            dst_ref=serves[kind].at[i - served[0], c - 2, slice(BLOCK, picked)],
+            send_sem=key_send.at[kind], recv_sem=wire_recv.at[len(served) + i - served[0], c - 2],
+            device_id={"kv": server}, device_id_type=MESH,
+        )
+
+    def root_copy(kind, some, t, passing=False):
+        own, buffer = buffers[kind]
+        part = slice(some[0], some[-1] + 1)
+        here = lambda slot: buffer.at[part, slice((slot - 1) * LANES, (slot - 1) * LANES + BLOCK)]
+        return pltpu.make_async_remote_copy(
+            src_ref=here(t - 1) if passing else own.at[part, slice(0, BLOCK)], dst_ref=here(t),
+            send_sem=key_send.at[kind], recv_sem=root_recv.at[kind, 1 if some is served else 0],
+            device_id={"kv": t}, device_id_type=MESH,
+        )
+
+    def query_copy(i):
+        n = i - served[0]
+        return pltpu.make_async_remote_copy(
+            src_ref=q_out.at[n], dst_ref=q_in.at[n, jnp.maximum(me - 2, 0)],
+            send_sem=wire_send.at[0], recv_sem=wire_recv.at[n, jnp.maximum(me - 2, 0)],
+            device_id={"kv": server}, device_id_type=MESH,
+        )
+
+    def query_arrived(i, c):
+        n = i - served[0]
+        space = q_in.at[n, c - 2]
+        pltpu.make_async_copy(space, space, wire_recv.at[n, c - 2]).wait()
+
+    def state_copy(i, c):
+        n = i - served[0]
+        return pltpu.make_async_remote_copy(
+            src_ref=state_out.at[n, c - 2], dst_ref=state_in.at[n],
+            send_sem=wire_send.at[0], recv_sem=wire_recv.at[n, 0],
+            device_id={"kv": c}, device_id_type=MESH,
+        )
+
+    everything = list(range(pairs))
+
+    @pl.when(me == 0)
+    def _():
+        wk_load.wait()
+        begin(k_acc, wk)
+        turn_tables()
+        wv_load.wait()
+        begin(v_acc, wv)
+        tok_copy.wait_recv()
+        make_keys(everything)
+        make_values(everything)
+        choose(0, 1)
+        for kind in range(2):
+            root_copy(kind, served, 1).start()
+        choose(0, 2)
+        for kind in range(2):
+            root_copy(kind, plain, 2).start()
+        choose(0, 3)
+
+        def pick(i):
+            for (_, buffer), got in zip(buffers, gather([(k_own, i), (v_own, i)], 1, 3)):
+                buffer[i] = got
+
+        for step in range(max(len(served), len(plain))):
+            for i in served[step : step + 1]:
+                pick(i)
+                for c in clients:
+                    for kind in range(2):
+                        serve_copy(kind, i, c).start()
+                for kind in range(2):
+                    row_copy(kind, i, 0, 1).start()
+            for i in plain[step : step + 1]:
+                pick(i)
+                for kind in range(2):
+                    for t in (2, 3):
+                        row_copy(kind, i, 0, t).start()
+        for kind in range(2):
+            root_copy(kind, plain, 1).start()
+            for i in plain:
+                row_copy(kind, i, 0, 1).start()
+        wq_load.wait()
+        begin(q_acc, wq)
+        make_queries(everything)
+
+    @pl.when(me == 1)
+    def _():
+        wk_load.wait()
+        begin(k_acc, wk)
+        turn_tables()
+        wv_load.wait()
+        begin(v_acc, wv)
+        tok_copy.wait_recv()
+
+        def pass_on(kind, t):
+            own, buffer = buffers[kind]
+            slot = slice((t - 1) * LANES, t * LANES)
+            for i, got in zip(plain, gather([(own, i) for i in plain], t, t)):
+                buffer[i, slot, :] = got
+            for i in plain:
+                row_copy(kind, i, 1, t).start()
+
+        make_keys(plain)
+        choose(1, 2)
+        pass_on(0, 2)
+        make_values(plain)
+        pass_on(1, 2)
+        choose(1, 3)
+        pass_on(0, 3)
+        pass_on(1, 3)
+        make_keys(served)
+        make_values(served)
+        for i in served:
+            for buffer, got in zip(serves, gather([(k_own, i), (v_own, i)], 2, 3)):
+                for c in clients:
+                    buffer[i - served[0], c - 2, LANES : 2 * LANES, :] = got[(c - 2) * LANES : (c - 1) * LANES]
+        wq_load.wait()
+        begin(q_acc, wq)
+        make_queries(everything)
+
+    @pl.when(me >= 2)
+    def _():
+        wq_load.wait()
+        begin(q_acc, wq)
+        turn_tables()
+        wk_load.wait()
+        begin(k_acc, wk)
+        tok_copy.wait_recv()
+        make_queries(served, True)
+        query_copy(served[0]).start()
+        make_keys(everything)
+        for i in served[1:]:
+            query_copy(i).start()
+
+        def pass_on(kind):
+            @pl.when(me == 2)
+            def _():
+                own, buffer = buffers[kind]
+                if kind == 0:
+                    choose(2, 3)
+                for i, got in zip(everything, gather([(own, i) for i in everything], 3, 3)):
+                    buffer[i, 2 * LANES :, :] = got
+                for i in served + plain:
+                    row_copy(kind, i, 2, 3).start()
+
+        pass_on(0)
+        wv_load.wait()
+        begin(v_acc, wv)
+        make_values(everything)
+        pass_on(1)
+        make_queries(plain)
+
+    chosen = chosen_ref[...]
+
+    def spread(hit):
+        keys = hit.shape[1]
+        blocks = hit.shape[0]
+        wide = jnp.broadcast_to(hit[:, None, :], (blocks, BLOCK, keys))
+        return wide.reshape(blocks * BLOCK, keys)
+
+    def scores_of(queries, keys):
+        return lax.dot_general(queries, keys, (((1,), (1,)), ((), ())), preferred_element_type=F32)
+
+    def lane_sums(weights):
+        return sum(weights[:, j : j + LANES] for j in range(0, weights.shape[1], LANES))
+
+    def twice(x):
+        return jnp.concatenate([x, x], axis=0)
+
+    listed = spread(listed_columns(chosen, me, rows))
+    bias = twice(jnp.where((listed > 0.5) & (col_i <= row_i), 0.0, MASKED))
+    for i in everything:
+        scores = scores_of(q2[i], k_own[i]) + bias
+        top = jnp.max(scores, axis=1, keepdims=True)
+        weights = jnp.exp(scores - top)
+        peak[i] = jnp.broadcast_to(top, peak.shape[1:])
+        total[i] = lane_sums(weights)
+        summed[i] = jnp.dot(weights.astype(BF16), v_own[i], preferred_element_type=F32)
+
+    def mask_of(wanted, holder):
+        hit = listed_columns(wanted, holder, rows)
+        pick = selection(hit, earlier, LANES)
+        got = lax.dot_general(
+            hit.astype(BF16), pick, (((1,), (1,)), ((), ())), preferred_element_type=F32
+        )
+        return jnp.where(spread(got) > 0.5, 0.0, MASKED)
+
+    @pl.when(me == server)
+    def _():
+        for c in clients:
+            for holder in range(2):
+                far_serve[c - 2, :, holder * LANES : (holder + 1) * LANES] = mask_of(lists[c - 2], holder)
+
+    @pl.when(me == 2)
+    def _():
+        for kind in range(2):
+            root_copy(kind, plain, 2).wait_recv()
+            root_copy(kind, plain, 3, True).start()
+
+    for d in range(1, devices):
+
+        @pl.when(me >= d)
+        def _(d=d):
+            far[:, (d - 1) * LANES : d * LANES] = mask_of(chosen, me - d)
+
+    def att_copy(i):
+        return pltpu.make_async_remote_copy(
+            src_ref=att_own.at[i], dst_ref=att_peer.at[i], send_sem=att_send.at[0],
+            recv_sem=att_recv.at[i], device_id={"tp": other}, device_id_type=MESH,
+        )
+
+    def finish(i, merged):
+        att_own[i] = merged.astype(BF16)
+        att_copy(i).start()
+
+    def by_head(result):
+        return jnp.where(lane < HEAD_DIM, result[:rows], result[rows:])
+
+    def product(i):
+        att_copy(i).wait_recv()
+        both = jnp.concatenate([att_own[i], att_peer[i]], axis=1)
+        weight = jnp.concatenate(
+            [
+                wo[pl.ds(pl.multiple_of((device * pairs + i) * LANES, LANES), LANES), :]
+                for device in (core, other)
+            ],
+            axis=0,
+        )
+        return jnp.dot(both, weight, preferred_element_type=F32)
+
+    def project(order, low, high):
+        for n in range(low, high):
+            got = product(order[n])
+            if n > 0:
+                got = mixed[...] + got
+            if n == pairs - 1:
+                out_ref[...] = got.astype(BF16)
+            else:
+                mixed[...] = got
+
+    def arrived(kind, i, count):
+        space = buffers[kind][1].at[i, slice(0, count)]
+        pltpu.make_async_copy(space, space, key_recv.at[kind, i]).wait()
+
+    def key_part(m, i, n):
+        arrived(0, i, m * picked - BLOCK)
+        keys = slice(0, m * LANES)
+        scores = scores_of(q2[i], k_rows[i, keys, :]) + twice(far[:, keys])
+        old = peak[i]
+        top = jnp.maximum(old, jnp.max(scores, axis=1, keepdims=True))
+        factor = jnp.exp(old - top)
+        weights = jnp.exp(scores - jnp.concatenate([top] * m, axis=1))
+        inverse = 1.0 / jnp.sum(total[i] * factor + lane_sums(weights), axis=1, keepdims=True)
+        summed[i] = summed[i] * (factor * inverse)
+        total[i] = jnp.broadcast_to(inverse, total.shape[1:])
+        weigh[n, :, keys] = weights.astype(BF16)
+
+    def value_part(m, i, n):
+        arrived(1, i, m * picked - BLOCK)
+        keys = slice(0, m * LANES)
+        after = jnp.dot(weigh[n, :, keys], v_rows[i, keys, :], preferred_element_type=F32)
+        finish(i, by_head(summed[i] + after * total[i]))
+
+    eye = lax.broadcasted_iota(jnp.int32, (LANES, LANES), 0) == lax.broadcasted_iota(jnp.int32, (LANES, LANES), 1)
+    strips = 2 * rows // LANES
+
+    def serve(i, c):
+        n = i - served[0]
+        query_arrived(i, c)
+        space = k_rows.at[i, slice(0, 2 * (picked - BLOCK))]
+        pltpu.make_async_copy(space, space, wire_recv.at[len(served) + n, c - 2]).wait()
+        for kind in range(2):
+            serves[kind][n, c - 2, :BLOCK, :] = buffers[kind][1][i, :BLOCK, :]
+        q = q_in[n, c - 2].astype(F32)
+        q = jnp.concatenate(
+            [jnp.where(lane < HEAD_DIM, q, 0.0), jnp.where(lane < HEAD_DIM, 0.0, q)], axis=0
+        ).astype(BF16)
+        scores = scores_of(q, k_serve[n, c - 2]) + twice(far_serve[c - 2])
+        top = jnp.max(scores, axis=1, keepdims=True)
+        weights = jnp.exp(scores - top)
+        mass = jnp.sum(lane_sums(weights), axis=1, keepdims=True)
+        result = jnp.dot(weights.astype(BF16), v_serve[n, c - 2], preferred_element_type=F32)
+        state_out[n, c - 2, :rows, :] = by_head(result * (1.0 / mass)).astype(BF16)
+        level = top + jnp.log(mass)
+        strip = jnp.concatenate(
+            [
+                jnp.sum(jnp.where(eye, level[j * LANES : (j + 1) * LANES], 0.0), axis=0, keepdims=True)
+                for j in range(strips)
+            ],
+            axis=0,
+        )
+        high = strip.astype(BF16).astype(F32)
+        middle = (strip - high).astype(BF16).astype(F32)
+        low = strip - high - middle
+        spare = jnp.zeros((state_out.shape[2] - rows - 3 * strips, LANES), F32)
+        state_out[n, c - 2, rows:, :] = jnp.concatenate([high, middle, low, spare], axis=0).astype(BF16)
+        state_copy(i, c).start()
+
+    def fold(i):
+        for kind in range(2):
+            arrived(kind, i, picked)
+        scores = scores_of(q2[i], k_rows[i, :LANES, :]) + twice(far[:, :LANES])
+        old = peak[i]
+        top = jnp.maximum(old, jnp.max(scores, axis=1, keepdims=True))
+        factor = jnp.exp(old - top)
+        weights = jnp.exp(scores - top)
+        peak[i] = top
+        total[i] = total[i] * factor + weights
+        summed[i] = summed[i] * factor + jnp.dot(
+            weights.astype(BF16), v_rows[i, :LANES, :], preferred_element_type=F32
+        )
+
+    def merge(i):
+        n = i - served[0]
+        mass = jnp.sum(total[i], axis=1, keepdims=True)
+        state_copy(i, 2).wait_recv()
+        tail = state_in[n, rows:, :].astype(F32)
+        strip = tail[:strips] + tail[strips : 2 * strips] + tail[2 * strips : 3 * strips]
+        level = jnp.concatenate(
+            [
+                jnp.sum(jnp.where(eye, strip[j : j + 1], 0.0), axis=1, keepdims=True)
+                for j in range(strips)
+            ],
+            axis=0,
+        )
+        old = peak[i]
+        top = jnp.maximum(old, level)
+        factor, share = jnp.exp(old - top), jnp.exp(level - top)
+        inverse = 1.0 / (mass * factor + share)
+        there = state_in[n, :rows, :].astype(F32)
+        finish(i, by_head(summed[i] * (factor * inverse)) + there * by_head(share * inverse))
+
+    wo_load.wait()
+
+    @pl.when(me == 0)
+    def _():
+        for i in everything:
+            finish(i, by_head(summed[i] / jnp.sum(total[i], axis=1, keepdims=True)))
+        project(everything, 0, pairs)
+
+    @pl.when(me == server)
+    def _():
+        for kind in range(2):
+            root_copy(kind, served, 1).wait_recv()
+        for i in served:
+            for c in clients:
+                serve(i, c)
+            key_part(1, i, 0)
+            value_part(1, i, 0)
+        order = served + plain
+        for kind in range(2):
+            root_copy(kind, plain, 1).wait_recv()
+        for n, i in enumerate(plain):
+            key_part(1, i, n)
+        project(order, 0, len(served))
+        for n, i in enumerate(plain):
+            value_part(1, i, n)
+        project(order, len(served), pairs)
+
+    for m in clients:
+
+        @pl.when(me == m)
+        def _(m=m):
+            if m == 3:
+                for i in served:
+                    fold(i)
+                root_copy(0, plain, 3).wait_recv()
+            for n, i in enumerate(plain):
+                key_part(m, i, n)
+            if m == 3:
+                root_copy(1, plain, 3).wait_recv()
+            for n, i in enumerate(plain):
+                value_part(m, i, n)
+            merge(served[0])
+            project(everything, 0, len(plain))
+            for i in served[1:]:
+                merge(i)
+            project(everything, len(plain), pairs)
+
+    def settle(space, semaphore):
+        pltpu.make_async_copy(space, space, semaphore).wait()
+
+    settle(att_own, att_send.at[0])
+    settle(tok_own, tok_send.at[0])
+    for m in range(1, devices):
+
+        @pl.when(me == m)
+        def _(m=m):
+            settle(lists.at[slice(0, m)], list_send.at[0])
+
+    @pl.when(me == server)
+    def _():
+        settle(state_out, wire_send.at[0])
+
+    @pl.when(me >= 2)
+    def _():
+        settle(q_out, wire_send.at[0])
+
+    fresh = picked - BLOCK
+    sent = {
+        0: [pairs * BLOCK + len(plain) * BLOCK + pairs * 3 * fresh],
+        1: [len(plain) * 2 * picked],
+        2: [len(plain) * BLOCK + pairs * picked],
+    }
+    width = (devices - 1) * LANES
+    for m, (count,) in sent.items():
+
+        @pl.when(me == m)
+        def _(count=count):
+            for kind in range(2):
+                buffer = buffers[kind][1]
+                whole = count // pairs
+                settle(buffer.at[:, slice(0, whole)], key_send.at[kind])
+
+
+def quad_call(tokens, query_weight, key_weight, value_weight, out_weight, chosen):
+    devices = 4
+    rows, half = tokens.shape
+    width, head_width = query_weight.shape
+    pairs = head_width // LANES
+    table = np.concatenate(rotary_tables(rows, devices), axis=0)
+    vmem = pl.BlockSpec(memory_space=pltpu.VMEM)
+    anywhere = pl.BlockSpec(memory_space=pl.ANY)
+    dma = pltpu.SemaphoreType.DMA
+    served = pairs // 2
+    others = devices - 1
+    strips = 2 * rows // LANES
+    state = rows + -(-3 * strips // 16) * 16
+    return pl.pallas_call(
+        quad_layer,
+        out_shape=pltpu.VMEM((rows, out_weight.shape[1]), BF16),
+        in_specs=[anywhere] * 7,
+        out_specs=vmem,
+        scratch_shapes=[
+            pltpu.VMEM(chosen.shape, jnp.int32),
+            pltpu.VMEM(table.shape, F32),
+            pltpu.VMEM((rows, half), BF16),
+            pltpu.VMEM((rows, half), BF16),
+            pltpu.VMEM((width, head_width), BF16),
+            pltpu.VMEM((width, head_width), BF16),
+            pltpu.VMEM((width, head_width), BF16),
+            pltpu.VMEM(out_weight.shape, BF16),
+            pltpu.VMEM((rows, head_width), F32),
+            pltpu.VMEM((rows, head_width), F32),
+            pltpu.VMEM((rows, head_width), F32),
+            pltpu.VMEM((pairs, rows, LANES), BF16),
+            pltpu.VMEM((pairs, rows, LANES), BF16),
+            pltpu.VMEM((pairs, 2 * rows, LANES), BF16),
+            pltpu.VMEM((others,) + chosen.shape, jnp.int32),
+            pltpu.VMEM((others * LANES, rows), BF16),
+            pltpu.VMEM((pairs, others * LANES, LANES), BF16),
+            pltpu.VMEM((pairs, others * LANES, LANES), BF16),
+            pltpu.VMEM((rows, others * LANES), F32),
+            pltpu.VMEM((pairs, 2 * rows, LANES), F32),
+            pltpu.VMEM((pairs, 2 * rows, LANES), F32),
+            pltpu.VMEM((pairs, 2 * rows, LANES), F32),
+            pltpu.VMEM((pairs, 2 * rows, others * LANES), BF16),
+            pltpu.VMEM((rows, out_weight.shape[1]), F32),
+            pltpu.VMEM((pairs, rows, LANES), BF16),
+            pltpu.VMEM((pairs, rows, LANES), BF16),
+            pltpu.VMEM((served, 2, 2 * LANES, LANES), BF16),
+            pltpu.VMEM((served, 2, 2 * LANES, LANES), BF16),
+            pltpu.VMEM((2, rows, 2 * LANES), F32),
+            pltpu.VMEM((served, rows, LANES), BF16),
+            pltpu.VMEM((served, 2, rows, LANES), BF16),
+            pltpu.VMEM((served, 2, state, LANES), BF16),
+            pltpu.VMEM((served, state, LANES), BF16),
+            dma((7,)),
+            dma((1,)),
+            dma((1,)),
+            dma((1,)),
+            dma((pairs,)),
+            dma((1,)),
+            dma((others,)),
+            dma((2,)),
+            dma((2, pairs)),
+            dma((2, 2)),
+            dma((1,)),
+            dma((2 * served, 2)),
+        ],
+        compiler_params=pltpu.CompilerParams(
+            collective_id=0, has_side_effects=True, vmem_limit_bytes=62 * 1024 * 1024
+        ),
+        name="layer",
+    )(chosen, jnp.asarray(table), tokens, query_weight, key_weight, value_weight, out_weight)
+
+
 def on_device(devices, tokens, query_weight, key_weight, value_weight, out_weight, chosen):
     rows, half = tokens.shape
     width, head_width = query_weight.shape
     pairs = head_width // LANES
     picked = CAP * BLOCK
+    if devices == 4 and pairs % 2 == 0:
+        return quad_call(tokens, query_weight, key_weight, value_weight, out_weight, chosen)
     row_table, base_table = rotary_tables(rows, devices)
     vmem = pl.BlockSpec(memory_space=pltpu.VMEM)
     anywhere = pl.BlockSpec(memory_space=pl.ANY)

time: 26.8 us -> 22.2 us (0.83)
  the two profiles are of different devices: /device:TPU:17 before, /device:TPU:25 now
where the time goes in v4:
time: 22.2 us; the launch traced here: 22 us
  Pallas kernels  21.2 us (95%)
  local copies, waits for them, and re-layouts  0.8 us (4%)
    pallas_call x1, Pallas kernels, quad_call(): pl.pallas_call(quad_layer, out_shape=pltpu.VMEM((rows, out_weight.shape[1...  21.2 us
    unnamed x1, local copies, waits for them, and re-layouts  0.8 us

profile of v4, /device:TPU:25, one launch (start us, length us, event | category | flops | bytes accessed | tf_op | source)
XLA Modules:
  0.0 22.0 jit_solution(1881408659104479142)
XLA Ops:
  0.0 21.2 %layer.1 = bf16[256,1024]{1,0:T(8,128)(2,1)S(1)} custom-call(s32[8,16]{1,0:T(8,128)} %chosen_hbm.1, f32[260,256]{1,0:T(8,128)} %constant.2.clone.tab_hbm, bf16[256,1024]{1,0:T(8,128)(2,1)} %tok_hbm.1, bf16[2048,512]{1,0:T(8,128)(2,1)} %wq_hbm.1, bf16[2048,512]{1,0:T(8,128)(2,1)} %wk_hbm.1, bf16[2048,512]{1,0:T(8,128)(2,1)} %wv_hbm.1, bf16[1024,1024]{1,0:T(8,128)(2,1)} %wo_hbm.1), custom_call_target="tpu_custom_call" | custom-call | tf_op jit(solution)/shard_map/layer/pallas_call | solution.py:944
  21.2 0.8 %copy.9 = bf16[256,1024]{1,0:T(8,128)(2,1)} copy(bf16[256,1024]{1,0:T(8,128)(2,1)S(1)} %layer.1) | data formatting | bytes 1048576
